TPU v7x, 32 devices: a whole 2x2x4 slice. The times are simulated.
32 devices in a mesh: fs: 4 (over y, x), tp: 8 (over z, core).
Axes of the slice: x: 2, y: 2, z: 4, core: 2. Of those that a mesh axis runs over, the one named last changes fastest.
Arguments:
- tokens: bfloat16 [4096, 2048], P(('fs', 'tp')), may hold values from -6 to 6
- up_weight: bfloat16 [2048, 4096], P('fs', 'tp'), may hold values from -0.125 to 0.125
- down_weight: bfloat16 [4096, 2048], P('tp', 'fs'), may hold values from -0.09375 to 0.09375
- cotangent: bfloat16 [4096, 2048], P(('fs', 'tp')), may hold values from -6 to 6
Outputs:
- input_grad: bfloat16 [4096, 2048], P(('fs', 'tp'))
- up_grad: float32 [2048, 4096], P('fs', 'tp')
- down_grad: float32 [4096, 2048], P('tp', 'fs')
All inputs are finite; a program needn't handle non-finite values.
Results may differ from a plain program's by a relative error of at most 0.018.
Values may be sent and summed in bfloat16 or wider, within the bound.
A program may use at most 128 MiB of HBM per device.

v0:
```python
import functools

import jax
import jax.numpy as jnp
from jax import lax
from jax.experimental import pallas as pl
from jax.experimental.pallas import tpu as pltpu
from jax.sharding import PartitionSpec as P

MESH = pl.DeviceIdType.MESH
BF16 = jnp.bfloat16
F32 = jnp.float32


def ring_index(p):
    q, b = p // 2, p % 2
    return 2 * q + b + (q % 2) * (1 - 2 * b)


def dot(a, b, ca, cb):
    return lax.dot_general(a, b, (((ca,), (cb,)), ((), ())), preferred_element_type=F32)


def kernel(
    nfs, nz, factor,
    tok_in, up_in, down_in, cot_in,
    dx_out, ug_out, dg_out,
    tok, cot, up, down, hid, dpre,
    dx_own, dx_send, dx_recv, dr_send, dr_recv,
    ug_own, dg_own, ug_send, ug_recv, dg_send, dg_recv,
    local_sem, zs, zr, ps, pr, ws, wr, gs, gr, xs, xr, rs, rr,
):
    fs, tp = lax.axis_index("fs"), lax.axis_index("tp")
    rows, width = tok_in.shape
    h = rows // 2
    block = 4 * h
    dl = up_in.shape[0]
    fl = up_in.shape[1]
    z, core = tp // 2, tp % 2
    pos = ring_index(fs)
    fwd = (fs, ((z + 1) % nz) * 2 + core)
    bwd = (fs, ((z + nz - 1) % nz) * 2 + core)
    mate = (fs, 2 * z + 1 - core)
    cw = (ring_index((pos + 1) % nfs), tp)
    ccw = (ring_index((pos + nfs - 1) % nfs), tp)

    def cols(o):
        return pl.ds(pl.multiple_of(o * dl, dl), dl)

    locals_ = [
        pltpu.make_async_copy(tok_in, tok.at[pl.ds(0, rows)], local_sem.at[0]),
        pltpu.make_async_copy(up_in, up.at[cols(fs)], local_sem.at[1]),
        pltpu.make_async_copy(down_in, down.at[:, cols(fs)], local_sem.at[2]),
        pltpu.make_async_copy(cot_in, cot.at[pl.ds(0, rows)], local_sem.at[3]),
    ]
    for c in locals_:
        c.start()
    barrier = pltpu.get_barrier_semaphore()
    peers = (fwd, bwd, mate, cw, ccw)
    for peer in peers:
        pl.semaphore_signal(barrier, inc=1, device_id=peer, device_id_type=MESH)
    pl.semaphore_wait(barrier, len(peers))
    for c in locals_:
        c.wait()

    sends = []

    def remote(src, dst, s, r, peer):
        c = pltpu.make_async_remote_copy(
            src_ref=src, dst_ref=dst, send_sem=s, recv_sem=r, device_id=peer, device_id_type=MESH
        )
        c.start()
        sends.append(c)
        return c

    bufs = (tok, cot)

    def z_send(k, a):
        out = []
        for d, peer in enumerate((fwd, bwd)):
            out.append(remote(
                bufs[a].at[pl.ds(k * block + d * h, h)],
                bufs[a].at[pl.ds((k + 1) * block + d * h, h)],
                zs.at[k, d, a], zr.at[k, d, a], peer,
            ))
        return out

    def mate_send(k, a):
        return remote(
            bufs[a].at[pl.ds(k * block, 2 * h)],
            bufs[a].at[pl.ds(k * block + 2 * h, 2 * h)],
            ps.at[k, a], pr.at[k, a], mate,
        )

    def w_send(k, half):
        a = ring_index((pos + nfs - k) % nfs)
        b = ring_index((pos + k) % nfs)
        n = dl // 2
        piece = up.at[pl.ds(pl.multiple_of(a * dl + half * n, n), n)]
        m = fl // 2
        other = down.at[pl.ds(half * m, m), cols(b)]
        return [
            remote(piece, piece, ws.at[k, half, 0], wr.at[k, half, 0], cw),
            remote(other, other, ws.at[k, half, 1], wr.at[k, half, 1], ccw),
        ]

    z_copy, w_copy, mate_copy = {}, {}, {}
    for a in range(2):
        z_copy[0, a] = z_send(0, a)
        w_copy[0, a] = w_send(0, a)
    for a in range(2):
        mate_copy[0, a] = mate_send(0, a)

    def hidden_block(s):
        here = pl.ds(s * block, block)
        active = jnp.maximum(dot(tok[here, :], up[...], 1, 0), 0.0)
        hid[here, :] = (active * active).astype(BF16)
        dh = dot(cot[here, :], down[...], 1, 1)
        dpre[here, :] = (2.0 * active * dh).astype(BF16)

    pair_copy = {}

    def dx_block(s):
        here = pl.ds(s * block, block)

        def tile(j, carry):
            c = cols(j)
            part = dot(dpre[here, :], up[c, :], 1, 1)
            dx_own[s, :, c] = part[: 2 * h]
            dx_send[s, :, c] = part[2 * h :].astype(BF16)
            return carry

        lax.fori_loop(0, nfs, tile, 0)
        pair_copy[s] = remote(dx_send.at[s], dx_recv.at[s], xs.at[s], xr.at[s], mate)

    x_copy = {}

    def x_step(r):
        s = r + 1 if r < nz - 1 else 0
        pair_copy[s].wait_recv()
        for d, peer in enumerate((fwd, bwd)):
            here = pl.ds(d * h, h)
            if r > 0:
                x_copy[r - 1, d].wait_recv()
            total = dx_own[s, here, :] + dx_recv[s, here, :].astype(F32)
            if r > 0:
                total = total + dr_recv[r - 1, here, :].astype(F32)
            if r < nz - 1:
                dr_send[r, here, :] = total.astype(BF16)
                x_copy[r, d] = remote(
                    dr_send.at[r, here], dr_recv.at[r, here], rs.at[r, d], rr.at[r, d], peer
                )
            else:
                dx_out[here, :] = total.astype(BF16)

    events = []
    for k in range(nfs - 1):
        for half in range(2):
            events.append(((2 * k + half + 1) * 1.5 / (nfs - 1), 1, k, half))
    for k in range(nz - 1):
        for a in range(2):
            events.append(((2 * k + a + 1) * 3.0 / (nz - 1), 0, k, a))
    events.sort()
    weights_left = 2 * (nfs - 1)
    ready = [0]

    def settle(s):
        for a in range(2):
            mate_copy[s, a].wait_recv()
        hidden_block(s)
        if s < nz - 1:
            dx_block(s)

    for _, kind, k, a in events:
        if kind == 1:
            for c in w_copy[k, a]:
                c.wait_recv()
            if k + 1 < nfs - 1:
                w_copy[k + 1, a] = w_send(k + 1, a)
            weights_left -= 1
        else:
            for c in z_copy[k, a]:
                c.wait_recv()
            if k + 1 < nz - 1:
                z_copy[k + 1, a] = z_send(k + 1, a)
            mate_copy[k + 1, a] = mate_send(k + 1, a)
            if a == 1:
                ready.append(k + 1)
        if weights_left == 0 and (kind, k) != (0, nz - 2):
            for s in ready:
                settle(s)
            ready = []
    for s in ready[:-1]:
        settle(s)
    x_step(0)
    settle(ready[-1])

    def up_term(r):
        o = ring_index((pos + nfs - r - 1) % nfs)
        return dot(tok[:, cols(o)], dpre[...], 0, 0)

    def down_term(r):
        o = ring_index((pos + r + 1) % nfs)
        return dot(hid[...], cot[:, cols(o)], 0, 0)

    g_copy = {}

    def g_send(r, half, which):
        n, m = dl // 2, fl // 2
        a, b = pl.ds(half * n, n), pl.ds(half * m, m)
        if which == 0:
            g_copy[r, half, 0] = remote(
                ug_send.at[r, a], ug_recv.at[r, a], gs.at[r, half, 0], gr.at[r, half, 0], cw
            )
        else:
            g_copy[r, half, 1] = remote(
                dg_send.at[r, b], dg_recv.at[r, b], gs.at[r, half, 1], gr.at[r, half, 1], ccw
            )

    def g_terms(r):
        ug_own[...] = up_term(r)
        dg_own[...] = down_term(r)

    def g_first():
        ug_send[0] = up_term(0).astype(BF16)
        for half in range(2):
            g_send(0, half, 0)
        dg_send[0] = down_term(0).astype(BF16)
        for half in range(2):
            g_send(0, half, 1)
        g_terms(1)

    def g_step(r, half):
        n, m = dl // 2, fl // 2
        a, b = pl.ds(half * n, n), pl.ds(half * m, m)
        g_copy[r - 1, half, 0].wait_recv()
        gu = ug_own[a, :] + ug_recv[r - 1, a, :].astype(F32)
        if r < nfs - 1:
            ug_send[r, a, :] = gu.astype(BF16)
            g_send(r, half, 0)
        else:
            ug_out[a, :] = gu * factor
        g_copy[r - 1, half, 1].wait_recv()
        gd = dg_own[b, :] + dg_recv[r - 1, b, :].astype(F32)
        if r < nfs - 1:
            dg_send[r, b, :] = gd.astype(BF16)
            g_send(r, half, 1)
        else:
            dg_out[b, :] = gd * factor

    g_first()
    dx_block(nz - 1)
    for r in range(1, max(nfs, nz)):
        if r < nfs:
            g_step(r, 0)
        if r < nz:
            x_step(r)
        if r < nfs:
            g_step(r, 1)
            if r < nfs - 1:
                g_terms(r + 1)
    for c in sends:
        c.wait_send()


def shards(nfs, ntp, tokens, up_weight, down_weight, cotangent):
    rows, width = tokens.shape
    dl, fl = up_weight.shape
    nz = ntp // 2
    whole = rows * ntp
    factor = 1.0 / (whole * nfs) ** 0.5
    dma = pltpu.SemaphoreType.DMA
    any_space = pl.BlockSpec(memory_space=pl.ANY)
    vmem = pl.BlockSpec(memory_space=pltpu.VMEM)
    return pl.pallas_call(
        functools.partial(kernel, nfs, nz, factor),
        out_shape=(
            jax.ShapeDtypeStruct((rows, width), BF16),
            jax.ShapeDtypeStruct((dl, fl), F32),
            jax.ShapeDtypeStruct((fl, dl), F32),
        ),
        in_specs=[any_space] * 4,
        out_specs=(vmem, vmem, vmem),
        scratch_shapes=[
            pltpu.VMEM((whole, width), BF16),
            pltpu.VMEM((whole, width), BF16),
            pltpu.VMEM((width, fl), BF16),
            pltpu.VMEM((fl, width), BF16),
            pltpu.VMEM((whole, fl), BF16),
            pltpu.VMEM((whole, fl), BF16),
            pltpu.VMEM((nz, rows, width), F32),
            pltpu.VMEM((nz, rows, width), BF16),
            pltpu.VMEM((nz, rows, width), BF16),
            pltpu.VMEM((nz - 1, rows, width), BF16),
            pltpu.VMEM((nz - 1, rows, width), BF16),
            pltpu.VMEM((dl, fl), F32),
            pltpu.VMEM((fl, dl), F32),
            pltpu.VMEM((nfs - 1, dl, fl), BF16),
            pltpu.VMEM((nfs - 1, dl, fl), BF16),
            pltpu.VMEM((nfs - 1, fl, dl), BF16),
            pltpu.VMEM((nfs - 1, fl, dl), BF16),
            dma((4,)),
            dma((nz - 1, 2, 2)), dma((nz - 1, 2, 2)),
            dma((nz, 2)), dma((nz, 2)),
            dma((nfs - 1, 2, 2)), dma((nfs - 1, 2, 2)),
            dma((nfs - 1, 2, 2)), dma((nfs - 1, 2, 2)),
            dma((nz,)), dma((nz,)),
            dma((nz - 1, 2)), dma((nz - 1, 2)),
        ],
        compiler_params=pltpu.CompilerParams(
            collective_id=0, has_side_effects=True, vmem_limit_bytes=67_000_000
        ),
    )(tokens, up_weight, down_weight, cotangent)


def solution(mesh):
    placed = (P(("fs", "tp"), None), P("fs", "tp"), P("tp", "fs"), P(("fs", "tp"), None))
    return jax.shard_map(
        functools.partial(shards, mesh.shape["fs"], mesh.shape["tp"]),
        mesh=mesh,
        in_specs=placed,
        out_specs=(P(("fs", "tp"), None), P("fs", "tp"), P("tp", "fs")),
        check_vma=False,
    )
```

profile of v0, /device:TPU:0, one launch (start us, length us, event | category | flops | bytes accessed | tf_op | source)
XLA Modules:
  0.0 119.9 jit_solution(12453583964212716785)
XLA Ops:
  0.6 114.7 %shard_map.67 = (bf16[128,2048]{1,0:T(8,128)(2,1)}, f32[512,512]{1,0:T(8,128)}, f32[512,512]{1,0:T(8,128)}) custom-call(bf16[128,2048]{1,0:T(8,128)(2,1)} %tok_in.1, bf16[512,512]{1,0:T(8,128)(2,1)} %up_in.1, bf16[512,512]{1,0:T(8,128)(2,1)} %down_in.1, bf16[128,2048]{1,0:T(8,128)(2,1)} %cot_in.1), custom_call_target="tpu_custom_call" | custom-call | tf_op jit(solution)/shard_map/pallas_call | solution.py:275
  115.4 0.0 copy-start.1
  115.4 2.0 %copy.10 = bf16[128,2048]{1,0:T(8,128)(2,1)} copy(bf16[128,2048]{1,0:T(8,128)(2,1)} %get-tuple-element.6) | data formatting | bytes 1048576
  117.4 0.0 copy-done.1
  117.4 0.0 copy-start
  117.4 1.0 copy.11
  118.3 0.6 copy-done
  119.0 1.0 copy.12
Async XLA Ops:
  115.4 2.0 %copy-start.1 = (f32[512,512]{1,0:T(8,128)S(1)}, f32[512,512]{1,0:T(8,128)}, u32[]{:S(2)}) copy-start(f32[512,512]{1,0:T(8,128)} %get-tuple-element.7) | copy-start | bytes 3145732
  117.4 1.6 %copy-start = (f32[512,512]{1,0:T(8,128)S(1)}, f32[512,512]{1,0:T(8,128)}, u32[]{:S(2)}) copy-start(f32[512,512]{1,0:T(8,128)} %get-tuple-element.8) | copy-start | bytes 3145732
where the time goes:
time: 120 us
  Pallas kernels  115 us (96%)
  local copies, waits for them, and re-layouts  4.55 us (4%)
    pallas_call x1, Pallas kernels, shards(): pl.pallas_call(functools.partial(kernel, nfs, nz, factor), out_shape=(jax...  115 us
    unnamed x7, local copies, waits for them, and re-layouts  4.55 us

commit v1 on v0

--- a/solution.py
+++ b/solution.py
@@ -313,10 +313,412 @@
     )(tokens, up_weight, down_weight, cotangent)
 
 
+def grid_kernel(
+    factor,
+    tok_in, up_in, down_in, cot_in,
+    dx_out, ug_out, dg_out,
+    tok, cot, up, down, up_home, down_home, hid, dpre, ug_acc, dg_acc,
+    gx_send, gx_recv, gz_send, gz_recv, gy_send, gm_send, gf_recv,
+    dx_own, dxm_send, dxm_recv, dxz_send, dxz_recv, dxy_send, dxy_recv,
+    local_sem, fys, fyr, fms, fmr, fzs, fzr, fxs, fxr,
+    tzs, tzr, tys, tyr, tms, tmr,
+    gxs, gxr, gzs, gzr, gys, gms, gfr,
+    ms, mr, dzs, dzr, dys, dyr,
+):
+    fs, tp = lax.axis_index("fs"), lax.axis_index("tp")
+    rows, width = tok_in.shape
+    dl, fl = up_in.shape
+    unit, hr, hd, hf = 2 * rows, rows // 2, dl // 2, fl // 2
+    x, y, z, c = fs % 2, fs // 2, tp // 2, tp % 2
+    p = z % 2
+    first = c == p
+    second = c != p
+    home = c == y
+    away = c != y
+    over = 2 * (1 - y) + x
+    mate = (fs, 2 * z + 1 - c)
+    xn = (2 * y + 1 - x, tp)
+    yn = (over, tp)
+    zn = (fs, 2 * (z + 1 - 2 * p) + c)
+    zf = (fs, 2 * ((z + 2) % 4) + c)
+
+    def cols(o):
+        return pl.ds(pl.multiple_of(o * dl, dl), dl)
+
+    own = jnp.logical_and(home, first)
+    locals_ = [
+        (pltpu.make_async_copy(up_in, up.at[cols(fs)], local_sem.at[0]), own),
+        (pltpu.make_async_copy(down_in, down.at[:, cols(fs)], local_sem.at[1]), own),
+        (pltpu.make_async_copy(up_in, up_home, local_sem.at[2]), jnp.logical_not(own)),
+        (pltpu.make_async_copy(down_in, down_home, local_sem.at[3]), jnp.logical_not(own)),
+        (pltpu.make_async_copy(tok_in, tok.at[pl.ds(0, rows)], local_sem.at[4]), None),
+        (pltpu.make_async_copy(cot_in, cot.at[pl.ds(0, rows)], local_sem.at[5]), None),
+    ]
+
+    def when(cond, f):
+        if cond is None:
+            f()
+        else:
+            pl.when(cond)(f)
+
+    for cp, cond in locals_:
+        when(cond, lambda cp=cp: cp.start())
+    barrier = pltpu.get_barrier_semaphore()
+    peers = (mate, xn, yn, (over, 2 * z + 1 - c), zn, zf)
+    for peer in peers:
+        pl.semaphore_signal(barrier, inc=1, device_id=peer, device_id_type=MESH)
+    pl.semaphore_wait(barrier, len(peers))
+    for cp, cond in locals_:
+        when(cond, lambda cp=cp: cp.wait())
+
+    sends = []
+
+    def remote(src, dst, s, r, peer, cond=None):
+        cp = pltpu.make_async_remote_copy(
+            src_ref=src, dst_ref=dst, send_sem=s, recv_sem=r, device_id=peer, device_id_type=MESH
+        )
+        sends.append((cp, cond))
+        return cp
+
+    def piece(o, q):
+        if q < 2:
+            return up.at[pl.ds(pl.multiple_of(o * dl + q * hd, hd), hd)]
+        return down.at[pl.ds((q - 2) * hf, hf), cols(o)]
+
+    def home_piece(q):
+        if q < 2:
+            return up_home.at[pl.ds(q * hd, hd)]
+        return down_home.at[pl.ds((q - 2) * hf, hf)]
+
+    bufs = (tok, cot)
+
+    def rows_of(j, u, shift=0):
+        return bufs[j % 2].at[pl.ds(u * unit + shift + (j // 2) * hr, hr)]
+
+    Q = range(4)
+    to_half = jnp.logical_and(home, second)
+    fy = [remote(home_piece(q), piece(fs, q), fys.at[q], fyr.at[q], (over, 2 * z + p), away) for q in Q]
+    fm = [remote(home_piece(q), piece(fs, q), fms.at[q], fmr.at[q], mate, to_half) for q in Q]
+    fz = [[remote(piece(o, q), piece(o, q), fzs.at[i, q], fzr.at[i, q], zn, first) for q in Q]
+          for i, o in enumerate((fs, over))]
+    fx = [[remote(piece(o, q), piece(o, q), fxs.at[i, q], fxr.at[i, q], xn) for q in Q]
+          for i, o in enumerate((fs, over))]
+    tz = [remote(rows_of(j, 0), rows_of(j, 1), tzs.at[j], tzr.at[j], zf) for j in Q]
+    ty = [[remote(rows_of(j, u), rows_of(j, u + 2), tys.at[u, j], tyr.at[u, j], yn) for j in Q]
+          for u in range(2)]
+    tm = [[remote(rows_of(j, u), rows_of(j, u, rows), tms.at[u, j], tmr.at[u, j], mate) for j in Q]
+          for u in range(4)]
+
+    @pl.when(away)
+    def _():
+        for q in Q:
+            fy[q].start()
+
+    @pl.when(to_half)
+    def _():
+        for q in Q:
+            fm[q].start()
+
+    @pl.when(second)
+    def _():
+        for j in Q:
+            tz[j].start()
+
+    for j in Q:
+        ty[0][j].start()
+    for j in Q:
+        tm[0][j].start()
+
+    @pl.when(first)
+    def _():
+        for q in Q:
+            pl.when(away)(lambda q=q: fm[q].wait_recv())
+            fz[0][q].start()
+            fx[0][q].start()
+        for q in Q:
+            fy[q].wait_recv()
+            fz[1][q].start()
+            fx[1][q].start()
+        for j in Q:
+            tz[j].start()
+        for j in Q:
+            ty[0][j].wait_recv()
+            tm[2][j].start()
+        for j in Q:
+            tz[j].wait_recv()
+            ty[1][j].start()
+            tm[1][j].start()
+
+    @pl.when(second)
+    def _():
+        for q in Q:
+            fz[0][q].wait_recv()
+            fx[0][q].start()
+            tz[q].wait_recv()
+            ty[1][q].start()
+            tm[1][q].start()
+        for q in Q:
+            fz[1][q].wait_recv()
+            fx[1][q].start()
+        for j in Q:
+            ty[0][j].wait_recv()
+            tm[2][j].start()
+
+    def hidden_block(u):
+        here = pl.ds(u * unit, unit)
+        active = jnp.maximum(dot(tok[here, :], up[...], 1, 0), 0.0)
+        hid[here, :] = (active * active).astype(BF16)
+        dh = dot(cot[here, :], down[...], 1, 1)
+        dpre[here, :] = (2.0 * active * dh).astype(BF16)
+
+    dxm = [remote(dxm_send.at[u], dxm_recv.at[u], ms.at[u], mr.at[u], mate) for u in range(4)]
+
+    def dx_block(u):
+        here = pl.ds(u * unit, unit)
+
+        def tile(j, carry):
+            o = cols(j)
+            part = dot(dpre[here, :], up[o, :], 1, 1)
+            dx_own[u, :, o] = part[:rows]
+            dxm_send[u, :, o] = part[rows:].astype(BF16)
+            return carry
+
+        lax.fori_loop(0, 4, tile, 0)
+        dxm[u].start()
+
+    def relay(j):
+        ty[1][j].wait_recv()
+        tm[3][j].start()
+
+    dxz = [remote(dxz_send.at[i], dxz_recv.at[i], dzs.at[i], dzr.at[i], zf) for i in range(2)]
+    dxy = remote(dxy_send, dxy_recv, dys.at[0], dyr.at[0], yn)
+
+    def dx_sum(u):
+        dxm[u].wait_recv()
+        return dx_own[u] + dxm_recv[u].astype(F32)
+
+    def dx_far(i):
+        dxz_send[i] = dx_sum(2 * i + 1).astype(BF16)
+        dxz[i].start()
+
+    for q in Q:
+        fx[0][q].wait_recv()
+        fx[1][q].wait_recv()
+    for j in Q:
+        tm[0][j].wait_recv()
+    hidden_block(0)
+    for j in Q:
+        tm[2][j].wait_recv()
+    hidden_block(2)
+    for j in Q:
+        tm[1][j].wait_recv()
+    hidden_block(1)
+    dx_block(1)
+    relay(0)
+    early = pl.ds(0, 3 * unit)
+    last = pl.ds(3 * unit, unit)
+
+    def ug_early(o, carry):
+        ug_acc[cols(o), :] = dot(tok[early, cols(o)], dpre[early, :], 0, 0)
+        return carry
+
+    def dg_early(o, carry):
+        dg_acc[:, cols(o)] = dot(hid[early, :], cot[early, cols(o)], 0, 0)
+        return carry
+
+    lax.fori_loop(0, 4, ug_early, 0)
+    relay(1)
+    dx_far(0)
+    lax.fori_loop(0, 4, dg_early, 0)
+    relay(2)
+    relay(3)
+    for j in Q:
+        tm[3][j].wait_recv()
+    hidden_block(3)
+
+    def ug_val(o):
+        return ug_acc[cols(o), :] + dot(tok[last, cols(o)], dpre[last, :], 0, 0)
+
+    def dg_val(o):
+        return dg_acc[:, cols(o)] + dot(hid[last, :], cot[last, cols(o)], 0, 0)
+
+    o_xy = 2 * (1 - y) + 1 - x
+    o_x = 2 * y + 1 - x
+    o_y = over
+    o_me = fs
+    gx = [remote(gx_send.at[i], gx_recv.at[i], gxs.at[i], gxr.at[i], xn, None if i < 6 else first)
+          for i in range(8)]
+    gz = [[remote(gz_send.at[i, s], gz_recv.at[i, s], gzs.at[i, s], gzr.at[i, s], zn, second)
+           if s == 0 or i >= 6 else None for s in range(2)] for i in range(8)]
+
+    def put_x(i, val, start=None):
+        for h in range(2):
+            gx_send[i + h] = val[h * hd : (h + 1) * hd].astype(BF16)
+        when(start, lambda: [gx[i + h].start() for h in range(2)] and None)
+
+    def put_z(s, o):
+        val = dg_val(o)
+
+        @pl.when(second)
+        def _():
+            for h in range(2):
+                gz_send[6 + h, s] = val[h * hf : (h + 1) * hf].astype(BF16)
+                gz[6 + h][s].start()
+
+        @pl.when(first)
+        def _():
+            dg_acc[:, cols(o)] = val
+
+    put_x(0, ug_val(o_xy))
+    put_z(0, o_xy)
+    put_x(2, ug_val(o_x))
+    dx_block(3)
+    put_z(1, o_y)
+    put_x(4, dg_val(o_x), second)
+    dx_far(1)
+    ug_acc[cols(o_y), :] = ug_val(o_y)
+
+    def acc_at(i):
+        h = i % 2
+        if i < 4:
+            o = o_y if i < 2 else o_me
+            return ug_acc[pl.ds(pl.multiple_of(o * dl + h * hd, hd), hd), :]
+        o = o_me if i < 6 else o_y
+        return dg_acc[pl.ds(h * hf, hf), cols(o)]
+
+    gy = [remote(gy_send.at[k], gf_recv.at[k], gys.at[k], gfr.at[k], (over, 2 * z + y), first) for k in Q]
+    to_mate = jnp.logical_and(first, away)
+    gm = [remote(gm_send.at[k], gf_recv.at[k], gms.at[k], gfr.at[k], mate, to_mate) for k in Q]
+    outs = (ug_out, dg_out)
+
+    def finish(i, total):
+        k = 2 * (i >= 4) + i % 2
+        if i in (0, 1, 6, 7):
+            gy_send[k] = total.astype(BF16)
+            gy[k].start()
+        else:
+            n = total.shape[0]
+
+            @pl.when(home)
+            def _():
+                outs[k // 2][pl.ds((k % 2) * n, n), :] = total * factor
+
+            @pl.when(away)
+            def _():
+                gm_send[k] = total.astype(BF16)
+                gm[k].start()
+
+    @pl.when(first)
+    def _():
+        for h in range(2):
+            gz[6 + h][0].wait_recv()
+            total = dg_acc[pl.ds(h * hf, hf), cols(o_xy)] + gz_recv[6 + h, 0].astype(F32)
+            gx_send[6 + h] = total.astype(BF16)
+            gx[6 + h].start()
+        gx[4].start()
+        gx[5].start()
+
+    def step(i):
+        gx[i].wait_recv()
+
+        @pl.when(second)
+        def _():
+            gz_send[i, 0] = (acc_at(i) + gx_recv[i].astype(F32)).astype(BF16)
+            gz[i][0].start()
+
+        @pl.when(first)
+        def _():
+            part = acc_at(i) + gx_recv[i].astype(F32)
+            gz[i][0].wait_recv()
+            finish(i, part + gz_recv[i, 0].astype(F32))
+
+    step(0)
+    ug_acc[cols(o_me), :] = ug_val(o_me)
+    step(1)
+    dg_acc[:, cols(o_me)] = dg_val(o_me)
+    dx_block(2)
+    dx_block(0)
+    step(2)
+    dxz[1].wait_recv()
+    dxy_send[...] = (dx_sum(2) + dxz_recv[1].astype(F32)).astype(BF16)
+    dxy.start()
+    step(3)
+
+    @pl.when(first)
+    def _():
+        for h in range(2):
+            i = 6 + h
+            gz[i][1].wait_recv()
+            gx[i].wait_recv()
+            finish(i, acc_at(i) + gz_recv[i, 1].astype(F32) + gx_recv[i].astype(F32))
+
+    step(4)
+    dxz[0].wait_recv()
+    near = dx_sum(0) + dxz_recv[0].astype(F32)
+    dxy.wait_recv()
+    dx_out[...] = (near + dxy_recv[...].astype(F32)).astype(BF16)
+    step(5)
+
+    @pl.when(jnp.logical_not(own))
+    def _():
+        for k in Q:
+            gy[k].wait_recv()
+            n = gf_recv.shape[1]
+            outs[k // 2][pl.ds((k % 2) * n, n), :] = gf_recv[k].astype(F32) * factor
+
+    for cp, cond in sends:
+        when(cond, lambda cp=cp: cp.wait_send())
+
+
+def grid_shards(nfs, ntp, tokens, up_weight, down_weight, cotangent):
+    rows, width = tokens.shape
+    dl, fl = up_weight.shape
+    factor = 1.0 / (rows * ntp * nfs) ** 0.5
+    mine = 8 * rows
+    hd = dl // 2
+    dma = pltpu.SemaphoreType.DMA
+    any_space = pl.BlockSpec(memory_space=pl.ANY)
+    vmem = pl.BlockSpec(memory_space=pltpu.VMEM)
+    V = pltpu.VMEM
+    return pl.pallas_call(
+        functools.partial(grid_kernel, factor),
+        out_shape=(
+            jax.ShapeDtypeStruct((rows, width), BF16),
+            jax.ShapeDtypeStruct((dl, fl), F32),
+            jax.ShapeDtypeStruct((fl, dl), F32),
+        ),
+        in_specs=[any_space] * 4,
+        out_specs=(vmem, vmem, vmem),
+        scratch_shapes=[
+            V((mine, width), BF16), V((mine, width), BF16),
+            V((width, fl), BF16), V((fl, width), BF16),
+            V((dl, fl), BF16), V((fl, dl), BF16),
+            V((mine, fl), BF16), V((mine, fl), BF16),
+            V((width, fl), F32), V((fl, width), F32),
+            V((8, hd, fl), BF16), V((8, hd, fl), BF16),
+            V((8, 2, hd, fl), BF16), V((8, 2, hd, fl), BF16),
+            V((4, hd, fl), BF16), V((4, hd, fl), BF16), V((4, hd, fl), BF16),
+            V((4, rows, width), F32), V((4, rows, width), BF16), V((4, rows, width), BF16),
+            V((2, rows, width), BF16), V((2, rows, width), BF16),
+            V((rows, width), BF16), V((rows, width), BF16),
+            dma((6,)), dma((4,)), dma((4,)), dma((4,)), dma((4,)),
+            dma((2, 4)), dma((2, 4)), dma((2, 4)), dma((2, 4)),
+            dma((4,)), dma((4,)), dma((2, 4)), dma((2, 4)), dma((4, 4)), dma((4, 4)),
+            dma((8,)), dma((8,)), dma((8, 2)), dma((8, 2)), dma((4,)), dma((4,)), dma((4,)),
+            dma((4,)), dma((4,)), dma((2,)), dma((2,)), dma((1,)), dma((1,)),
+        ],
+        compiler_params=pltpu.CompilerParams(
+            collective_id=0, has_side_effects=True, vmem_limit_bytes=67_000_000
+        ),
+    )(tokens, up_weight, down_weight, cotangent)
+
+
 def solution(mesh):
     placed = (P(("fs", "tp"), None), P("fs", "tp"), P("tp", "fs"), P(("fs", "tp"), None))
+    fs, tp = mesh.shape["fs"], mesh.shape["tp"]
+    body = grid_shards if (fs, tp) == (4, 8) else shards
     return jax.shard_map(
-        functools.partial(shards, mesh.shape["fs"], mesh.shape["tp"]),
+        functools.partial(body, mesh.shape["fs"], mesh.shape["tp"]),
         mesh=mesh,
         in_specs=placed,
         out_specs=(P(("fs", "tp"), None), P("fs", "tp"), P("tp", "fs")),

time: 120 us -> 136 us (1.13)
  Pallas kernels: 115 us -> 131 us
    pallas_call x1, Pallas kernels: 115 us -> 131 us  [grid_shards(): pl.pallas_call(functools.partial(grid_kernel, factor), out_shape=(jax.Sha...]
where the time goes in v1:
time: 136 us
  Pallas kernels  131 us (96%)
  local copies, waits for them, and re-layouts  4.55 us (3%)
    pallas_call x1, Pallas kernels, grid_shards(): pl.pallas_call(functools.partial(grid_kernel, factor), out_shape=(jax.Sha...  131 us
    unnamed x7, local copies, waits for them, and re-layouts  4.55 us

profile of v1, /device:TPU:0, one launch (start us, length us, event | category | flops | bytes accessed | tf_op | source)
XLA Modules:
  0.0 136.0 jit_solution(5613183303977519709)
XLA Ops:
  0.6 130.9 %shard_map.67 = (bf16[128,2048]{1,0:T(8,128)(2,1)}, f32[512,512]{1,0:T(8,128)}, f32[512,512]{1,0:T(8,128)}) custom-call(bf16[128,2048]{1,0:T(8,128)(2,1)} %tok_in.1, bf16[512,512]{1,0:T(8,128)(2,1)} %up_in.1, bf16[512,512]{1,0:T(8,128)(2,1)} %down_in.1, bf16[128,2048]{1,0:T(8,128)(2,1)} %cot_in.1), custom_call_target="tpu_custom_call" | custom-call | tf_op jit(solution)/shard_map/pallas_call | solution.py:683
  131.5 0.0 copy-start.1
  131.5 2.0 %copy.10 = bf16[128,2048]{1,0:T(8,128)(2,1)} copy(bf16[128,2048]{1,0:T(8,128)(2,1)} %get-tuple-element.6) | data formatting | bytes 1048576
  133.5 0.0 copy-done.1
  133.5 0.0 copy-start
  133.5 1.0 copy.11
  134.4 0.6 copy-done
  135.1 1.0 copy.12
Async XLA Ops:
  131.5 2.0 %copy-start.1 = (f32[512,512]{1,0:T(8,128)S(1)}, f32[512,512]{1,0:T(8,128)}, u32[]{:S(2)}) copy-start(f32[512,512]{1,0:T(8,128)} %get-tuple-element.7) | copy-start | bytes 3145732
  133.5 1.6 %copy-start = (f32[512,512]{1,0:T(8,128)S(1)}, f32[512,512]{1,0:T(8,128)}, u32[]{:S(2)}) copy-start(f32[512,512]{1,0:T(8,128)} %get-tuple-element.8) | copy-start | bytes 3145732

commit v2 on v0

--- a/solution.py
+++ b/solution.py
@@ -313,10 +313,417 @@
     )(tokens, up_weight, down_weight, cotangent)
 
 
+def line_kernel(
+    factor, give,
+    tok_in, up_in, down_in, cot_in,
+    dx_out, ug_out, dg_out,
+    tok, cot, up, down, up_give, down_give, hid, dpre, ug_acc, dg_acc,
+    ug_send, ug_recv, dg_send, dg_recv, ug_back, dg_back, ug_home, dg_home,
+    dx_own, dxm_send, dxm_recv, dxz_send, dxz_recv,
+    local_sem, exs, exr, wxs, wxr, wys, wyr, ts, tr, tms, tmr,
+    ms, mr, dzs, dzr, gs, gr, bs, br,
+):
+    fs, tp = lax.axis_index("fs"), lax.axis_index("tp")
+    rows, width = tok_in.shape
+    dl, fl = up_in.shape
+    unit, hr, hd = 2 * rows, rows // 2, dl // 2
+    x, y, z, c = fs % 2, fs // 2, tp // 2, tp % 2
+    high = z // 2
+    toward = 1 - 2 * high
+    at_end = z % 3 == 0
+    fx_, fy_, fd_ = 2 * y + 1 - x, 2 * (1 - y) + x, 2 * (1 - y) + 1 - x
+    mate = (fs, 2 * z + 1 - c)
+    xn, yn = (fx_, tp), (fy_, tp)
+    inner = (fs, 2 * (z + toward) + c)
+    outer = (fs, 2 * jnp.maximum(z - toward, 0) + c)
+    across = (fs, 2 * (3 - z) + c)
+    Q = range(4)
+
+    def cols(o):
+        return pl.ds(pl.multiple_of(o * dl, dl), dl)
+
+    bufs = (tok, cot)
+
+    def body(end):
+        nf = fl - give if end else fl + give
+        hf = nf // 2
+        nown = fl - give if end else fl
+        units = slice(0, nf)
+        locals_ = [
+            pltpu.make_async_copy(up_in.at[:, pl.ds(0, nown)], up.at[cols(fs), pl.ds(0, nown)], local_sem.at[0]),
+            pltpu.make_async_copy(down_in.at[pl.ds(0, nown)], down.at[pl.ds(0, nown), cols(fs)], local_sem.at[1]),
+            pltpu.make_async_copy(tok_in, tok.at[pl.ds(0, rows)], local_sem.at[2]),
+            pltpu.make_async_copy(cot_in, cot.at[pl.ds(0, rows)], local_sem.at[3]),
+        ]
+        if end:
+            locals_ += [
+                pltpu.make_async_copy(up_in.at[:, pl.ds(nown, give)], up_give, local_sem.at[4]),
+                pltpu.make_async_copy(down_in.at[pl.ds(nown, give)], down_give, local_sem.at[5]),
+            ]
+        for cp in locals_:
+            cp.start()
+        barrier = pltpu.get_barrier_semaphore()
+        peers = (mate, xn, yn, inner, across) if end else (mate, xn, yn, inner, outer)
+        for peer in peers:
+            pl.semaphore_signal(barrier, inc=1, device_id=peer, device_id_type=MESH)
+        pl.semaphore_wait(barrier, len(peers))
+        for cp in locals_:
+            cp.wait()
+
+        sends = []
+
+        def remote(src, dst, s, r, peer):
+            return pltpu.make_async_remote_copy(
+                src_ref=src, dst_ref=dst, send_sem=s, recv_sem=r, device_id=peer, device_id_type=MESH
+            )
+
+        def go(cp):
+            cp.start()
+            sends.append(cp)
+
+        def piece(o, q):
+            if q < 2:
+                return up.at[pl.ds(pl.multiple_of(o * dl + q * hd, hd), hd), pl.ds(0, nown)]
+            if q < 4:
+                return down.at[pl.ds((q - 2) * (nown // 2), nown // 2), cols(o)]
+            if q == 4:
+                return up.at[cols(o), pl.ds(fl, give)]
+            return down.at[pl.ds(fl, give), cols(o)]
+
+        pieces = Q if end else range(6)
+        wx = [[remote(piece(o, q), piece(o, q), wxs.at[i, q], wxr.at[i, q], xn) for q in pieces]
+              for i, o in enumerate((fs, fy_))]
+        wy = [[remote(piece(o, q), piece(o, q), wys.at[i, q], wyr.at[i, q], yn) for q in pieces]
+              for i, o in enumerate((fs, fx_))]
+
+        def rows_of(j, u, shift=0):
+            return bufs[j % 2].at[pl.ds(u * unit + shift + (j // 2) * hr, hr)]
+
+        def t_send(flow, j, u, v, peer):
+            go(remote(rows_of(j, u), rows_of(j, v), ts.at[flow, j], tr.at[v, j], peer))
+
+        def t_wait(u, j):
+            remote(rows_of(j, u), rows_of(j, u), ts.at[0, j], tr.at[u, j], mate).wait_recv()
+
+        tm = [[remote(rows_of(j, u), rows_of(j, u, rows), tms.at[u, j], tmr.at[u, j], mate) for j in Q]
+              for u in range(4)]
+
+        def w_got(q):
+            wx[0][q].wait_recv()
+            if q % 2 == 0:
+                go(wy[1][q])
+            wy[0][q].wait_recv()
+            if q % 2:
+                go(wx[1][q])
+
+        ex = (remote(up_give, up.at[cols(fs), pl.ds(fl, give)], exs.at[0], exr.at[0], inner),
+              remote(down_give, down.at[pl.ds(fl, give), cols(fs)], exs.at[1], exr.at[1], inner))
+
+        def hidden_block(u):
+            here = pl.ds(u * unit, unit)
+            active = jnp.maximum(dot(tok[here, :], up[:, units], 1, 0), 0.0)
+            hid[here, units] = (active * active).astype(BF16)
+            dh = dot(cot[here, :], down[units, :], 1, 1)
+            dpre[here, units] = (2.0 * active * dh).astype(BF16)
+
+        dxm = [remote(dxm_send.at[u], dxm_recv.at[u], ms.at[u], mr.at[u], mate) for u in range(4)]
+
+        def dx_block(u):
+            here = pl.ds(u * unit, unit)
+
+            def tile(j, carry):
+                o = cols(j)
+                part = dot(dpre[here, units], up[o, units], 1, 1)
+                dx_own[u, :, o] = part[:rows]
+                dxm_send[u, :, o] = part[rows:].astype(BF16)
+                return carry
+
+            lax.fori_loop(0, 4, tile, 0)
+            go(dxm[u])
+
+        def dx_sum(u):
+            dxm[u].wait_recv()
+            return dx_own[u] + dxm_recv[u].astype(F32)
+
+        def z_wait(slot):
+            remote(dxz_send.at[0], dxz_recv.at[slot], dzs.at[0], dzr.at[slot], mate).wait_recv()
+            return dxz_recv[slot].astype(F32)
+
+        def z_send(i, value, slot, peer):
+            dxz_send[i] = value.astype(BF16)
+            go(remote(dxz_send.at[i], dxz_recv.at[slot], dzs.at[i], dzr.at[slot], peer))
+
+        def ready(u):
+            for j in Q:
+                tm[u][j].wait_recv()
+            hidden_block(u)
+
+        if end:
+            for cp in ex:
+                go(cp)
+            for q in Q:
+                go(wx[0][q])
+                go(wy[0][q])
+            for j in Q:
+                t_send(0, j, 0, 1, inner)
+            for j in Q:
+                go(tm[0][j])
+            for j in Q:
+                w_got(j)
+                t_wait(1, j)
+                go(tm[1][j])
+            for q in Q:
+                (wy if q % 2 else wx)[1][q ^ 1].wait_recv()
+            ready(0)
+            ready(1)
+            dx_block(1)
+            t_wait(2, 0)
+            go(tm[2][0])
+            z_send(0, dx_sum(1), 0, inner)
+            for j in (1, 2, 3):
+                t_wait(2, j)
+                go(tm[2][j])
+            ready(2)
+            dx_block(2)
+            t_wait(3, 0)
+            go(tm[3][0])
+            z_send(1, dx_sum(2), 1, inner)
+        else:
+            for q in Q:
+                go(wx[0][q])
+                go(wy[0][q])
+            for j in Q:
+                t_send(0, j, 0, 1, outer)
+                t_send(1, j, 0, 2, inner)
+            for j in Q:
+                go(tm[0][j])
+            for i in range(2):
+                ex[i].wait_recv()
+                go(wx[0][4 + i])
+                go(wy[0][4 + i])
+            for j in Q:
+                t_wait(1, j)
+                t_send(2, j, 1, 3, inner)
+                go(tm[1][j])
+                t_wait(2, j)
+                t_send(3, j, 2, 2, outer)
+                go(tm[2][j])
+                w_got(j)
+            w_got(4)
+            w_got(5)
+            for j in (0, 1, 2):
+                t_wait(3, j)
+                t_send(4, j, 3, 3, outer)
+                go(tm[3][j])
+            for q in pieces:
+                (wy if q % 2 else wx)[1][q ^ 1].wait_recv()
+            ready(0)
+            ready(1)
+            t_wait(3, 3)
+            t_send(4, 3, 3, 3, outer)
+            go(tm[3][3])
+            ready(2)
+
+        early = pl.ds(0, 3 * unit)
+        last = pl.ds(3 * unit, unit)
+
+        def ug_early(o, carry):
+            ug_acc[cols(o), units] = dot(tok[early, cols(o)], dpre[early, units], 0, 0)
+            return carry
+
+        def dg_early(o, carry):
+            dg_acc[units, cols(o)] = dot(hid[early, units], cot[early, cols(o)], 0, 0)
+            return carry
+
+        if end:
+            lax.fori_loop(0, 4, ug_early, 0)
+            lax.fori_loop(0, 4, dg_early, 0)
+            dx_block(0)
+            for j in (1, 2, 3):
+                t_wait(3, j)
+                go(tm[3][j])
+        ready(3)
+
+        def buf(pair, k, q):
+            up_buf, down_buf = pair
+            if q < 2:
+                return up_buf.at[k, q, :, pl.ds(0, nf)]
+            return down_buf.at[k, q - 2, pl.ds(0, hf)]
+
+        out_bufs, in_bufs = (ug_send, dg_send), (ug_recv, dg_recv)
+
+        def g_copy(k, q):
+            over_x = k == 1 or (k == 0 and q % 2 == 0)
+            return remote(buf(out_bufs, k, q), buf(in_bufs, k, q), gs.at[k, q], gr.at[k, q], xn if over_x else yn)
+
+        g = [[g_copy(k, q) for q in Q] for k in range(3)]
+
+        def acc_of(o, q):
+            if q < 2:
+                return ug_acc, pl.ds(pl.multiple_of(o * dl + q * hd, hd), hd), units
+            return dg_acc, pl.ds((q - 2) * hf, hf), cols(o)
+
+        def g_put(k, q, value):
+            dst = buf(out_bufs, k, q)
+            dst[...] = value.astype(BF16)
+            go(g[k][q])
+
+        def terms(o, p):
+            part = last if end else slice(None)
+            if p == 0:
+                val = dot(tok[part, cols(o)], dpre[part, units], 0, 0)
+                if end:
+                    val = val + ug_acc[cols(o), units]
+                return val[:hd], val[hd:]
+            val = dot(hid[part, units], cot[part, cols(o)], 0, 0)
+            if end:
+                val = val + dg_acc[units, cols(o)]
+            return val[:hf], val[hf:]
+
+        def keep(o, q, value):
+            ref, a, b = acc_of(o, q)
+            ref[a, b] = value
+
+        for p in range(2):
+            for h, v in enumerate(terms(fd_, p)):
+                g_put(0, 2 * p + h, v)
+        for p in range(2):
+            even, odd = terms(fx_, p)
+            g_put(1, 2 * p, even)
+            keep(fx_, 2 * p + 1, odd)
+            even, odd = terms(fy_, p)
+            g_put(2, 2 * p + 1, odd)
+            keep(fy_, 2 * p, even)
+        dx_block(3)
+
+        def pass_on(q):
+            g[0][q].wait_recv()
+            k, o = (1, fx_) if q % 2 else (2, fy_)
+            ref, a, b = acc_of(o, q)
+            g_put(k, q, ref[a, b] + buf(in_bufs, 0, q)[...].astype(F32))
+
+        if not end:
+            z_send(1, dx_sum(3), 3, inner)
+        pass_on(0)
+        pass_on(1)
+        if end:
+            z_send(2, dx_sum(3), 1, across)
+        for p in range(2):
+            for h, v in enumerate(terms(fs, p)):
+                keep(fs, 2 * p + h, v)
+        pass_on(2)
+        pass_on(3)
+        if not end:
+            dx_block(2)
+            dx_block(1)
+            dx_block(0)
+            z_send(0, dx_sum(2) + z_wait(1), 2, inner)
+            z_send(2, dx_sum(1) + z_wait(3), 0, outer)
+
+        back = (remote(ug_back, ug_home, bs.at[0], br.at[0], outer),
+                remote(dg_back, dg_home, bs.at[1], br.at[1], outer))
+
+        def finish(q):
+            ref, a, b = acc_of(fs, q)
+            total = ref[a, b]
+            for k in (1, 2):
+                g[k][q].wait_recv()
+                total = total + buf(in_bufs, k, q)[...].astype(F32)
+            if q < 2:
+                r = pl.ds(q * hd, hd)
+                ug_out[r, pl.ds(0, nown)] = total[:, :nown] * factor
+                if not end:
+                    ug_back[r, :] = total[:, nown:].astype(BF16)
+            else:
+                n = min(nown - (q - 2) * hf, hf)
+                dg_out[pl.ds((q - 2) * hf, n), :] = total[:n] * factor
+                if n < hf:
+                    dg_back[...] = total[n:].astype(BF16)
+
+        for q in (0, 1):
+            finish(q)
+        if not end:
+            go(back[0])
+        for q in (2, 3):
+            finish(q)
+        if not end:
+            go(back[1])
+            near = dx_sum(0) + z_wait(0)
+            dx_out[...] = (near + z_wait(2)).astype(BF16)
+        else:
+            near = dx_sum(0) + z_wait(0)
+            dx_out[...] = (near + z_wait(1)).astype(BF16)
+            back[0].wait_recv()
+            ug_out[:, pl.ds(nown, give)] = ug_home[...].astype(F32) * factor
+            back[1].wait_recv()
+            dg_out[pl.ds(nown, give), :] = dg_home[...].astype(F32) * factor
+        for cp in sends:
+            cp.wait_send()
+
+    pl.when(at_end)(lambda: body(True))
+    pl.when(jnp.logical_not(at_end))(lambda: body(False))
+
+
+def put_out(n, *refs):
+    copies = [pltpu.make_async_copy(refs[i], refs[n + i], refs[2 * n].at[i]) for i in range(n)]
+    for cp in copies:
+        cp.start()
+    for cp in copies:
+        cp.wait()
+
+
+def line_shards(nfs, ntp, tokens, up_weight, down_weight, cotangent):
+    rows, width = tokens.shape
+    dl, fl = up_weight.shape
+    factor = 1.0 / (rows * ntp * nfs) ** 0.5
+    mine = ntp * rows
+    give = fl // 4
+    most = fl + give
+    hd, hf = dl // 2, most // 2
+    dma = pltpu.SemaphoreType.DMA
+    any_space = pl.BlockSpec(memory_space=pl.ANY)
+    vmem = pl.BlockSpec(memory_space=pltpu.VMEM)
+    V = pltpu.VMEM
+    results = pl.pallas_call(
+        functools.partial(line_kernel, factor, give),
+        out_shape=(V((rows, width), BF16), V((dl, fl), F32), V((fl, dl), F32)),
+        in_specs=[any_space] * 4,
+        out_specs=(vmem, vmem, vmem),
+        scratch_shapes=[
+            V((mine, width), BF16), V((mine, width), BF16),
+            V((width, most), BF16), V((most, width), BF16),
+            V((dl, give), BF16), V((give, dl), BF16),
+            V((mine, most), BF16), V((mine, most), BF16),
+            V((width, most), F32), V((most, width), F32),
+            V((3, 2, hd, most), BF16), V((3, 2, hd, most), BF16),
+            V((3, 2, hf, dl), BF16), V((3, 2, hf, dl), BF16),
+            V((dl, give), BF16), V((give, dl), BF16), V((dl, give), BF16), V((give, dl), BF16),
+            V((4, rows, width), F32), V((4, rows, width), BF16), V((4, rows, width), BF16),
+            V((3, rows, width), BF16), V((4, rows, width), BF16),
+            dma((6,)), dma((2,)), dma((2,)), dma((2, 6)), dma((2, 6)), dma((2, 6)), dma((2, 6)),
+            dma((5, 4)), dma((4, 4)), dma((4, 4)), dma((4, 4)),
+            dma((4,)), dma((4,)), dma((3,)), dma((4,)), dma((3, 4)), dma((3, 4)), dma((2,)), dma((2,)),
+        ],
+        compiler_params=pltpu.CompilerParams(
+            collective_id=0, has_side_effects=True, vmem_limit_bytes=60_000_000
+        ),
+    )(tokens, up_weight, down_weight, cotangent)
+    return pl.pallas_call(
+        functools.partial(put_out, len(results)),
+        out_shape=tuple(jax.ShapeDtypeStruct(r.shape, r.dtype) for r in results),
+        in_specs=[vmem] * len(results),
+        out_specs=(any_space,) * len(results),
+        scratch_shapes=[dma((3,))],
+        compiler_params=pltpu.CompilerParams(vmem_limit_bytes=8_000_000),
+    )(*results)
+
+
 def solution(mesh):
     placed = (P(("fs", "tp"), None), P("fs", "tp"), P("tp", "fs"), P(("fs", "tp"), None))
+    fs, tp = mesh.shape["fs"], mesh.shape["tp"]
+    body = line_shards if (fs, tp) == (4, 8) else shards
     return jax.shard_map(
-        functools.partial(shards, mesh.shape["fs"], mesh.shape["tp"]),
+        functools.partial(body, mesh.shape["fs"], mesh.shape["tp"]),
         mesh=mesh,
         in_specs=placed,
         out_specs=(P(("fs", "tp"), None), P("fs", "tp"), P("tp", "fs")),

time: 120 us -> 114 us (0.950)
  local copies, waits for them, and re-layouts: 4.55 us -> 0 us
  Pallas kernels: 115 us -> 113 us
    unnamed x7 -> x0, local copies, waits for them, and re-layouts: 4.55 us -> none
    pallas_call x1 -> x2, Pallas kernels: 115 us -> 113 us  [the longest x1 111 us: line_shards(): pl.pallas_call(functools.partial(line_kernel, factor, give), out_shape=(V...]
where the time goes in v2:
time: 114 us
  Pallas kernels  113 us (99%)
    pallas_call x1, Pallas kernels, line_shards(): pl.pallas_call(functools.partial(line_kernel, factor, give), out_shape=(V...  111 us

profile of v2, /device:TPU:0, one launch (start us, length us, event | category | flops | bytes accessed | tf_op | source)
XLA Modules:
  0.0 113.6 jit_solution(10696703744973828333)
XLA Ops:
  0.6 111.3 %shard_map.67 = (bf16[128,2048]{1,0:T(8,128)(2,1)S(1)}, f32[512,512]{1,0:T(8,128)S(1)}, f32[512,512]{1,0:T(8,128)S(1)}) custom-call(bf16[128,2048]{1,0:T(8,128)(2,1)} %tok_in.1, bf16[512,512]{1,0:T(8,128)(2,1)} %up_in.1, bf16[512,512]{1,0:T(8,128)(2,1)} %down_in.1, bf16[128,2048]{1,0:T(8,128)(2,1)} %cot_in.1), custom_call_target="tpu_custom_call" | custom-call | tf_op jit(solution)/shard_map/pallas_call | solution.py:687
  111.9 1.5 %shard_map.68 = (bf16[128,2048]{1,0:T(8,128)(2,1)}, f32[512,512]{1,0:T(8,128)}, f32[512,512]{1,0:T(8,128)}) custom-call(bf16[128,2048]{1,0:T(8,128)(2,1)S(1)} %get-tuple-element.6.refs_0_, f32[512,512]{1,0:T(8,128)S(1)} %get-tuple-element.7.refs_1_, f32[512,512]{1,0:T(8,128)S(1)} %get-tuple-element.8.refs_2_), custom_call_target="tpu_custom_call" | custom-call | tf_op jit(solution)/shard_map/pallas_call | solution.py:711

commit v3 on v2

--- a/solution.py
+++ b/solution.py
@@ -336,7 +336,7 @@
     xn, yn = (fx_, tp), (fy_, tp)
     inner = (fs, 2 * (z + toward) + c)
     outer = (fs, 2 * jnp.maximum(z - toward, 0) + c)
-    across = (fs, 2 * (3 - z) + c)
+    beyond = (fs, 2 * (z + 2 * toward) + c)
     Q = range(4)
 
     def cols(o):
@@ -363,7 +363,7 @@
         for cp in locals_:
             cp.start()
         barrier = pltpu.get_barrier_semaphore()
-        peers = (mate, xn, yn, inner, across) if end else (mate, xn, yn, inner, outer)
+        peers = (mate, xn, yn, inner, beyond) if end else (mate, xn, yn, inner, beyond, outer)
         for peer in peers:
             pl.semaphore_signal(barrier, inc=1, device_id=peer, device_id_type=MESH)
         pl.semaphore_wait(barrier, len(peers))
@@ -494,35 +494,79 @@
                 go(wy[0][q])
             for j in Q:
                 t_send(0, j, 0, 1, outer)
-                t_send(1, j, 0, 2, inner)
+            for j in (0, 1):
+                t_send(1, j, 0, 3, inner)
             for j in Q:
                 go(tm[0][j])
             for i in range(2):
                 ex[i].wait_recv()
                 go(wx[0][4 + i])
                 go(wy[0][4 + i])
-            for j in Q:
+
+            def from_end(j):
                 t_wait(1, j)
-                t_send(2, j, 1, 3, inner)
+                t_send(2, j, 1, 2, inner)
                 go(tm[1][j])
+
+            def from_middle(j):
+                t_wait(3, j)
+                go(tm[3][j])
+
+            def from_far(j):
                 t_wait(2, j)
-                t_send(3, j, 2, 2, outer)
+                t_send(4, j, 2, 2, outer)
                 go(tm[2][j])
-                w_got(j)
+
+            from_end(0)
+            w_got(0)
+            from_end(1)
+            from_middle(0)
+            from_middle(1)
+            w_got(1)
+            from_end(2)
+            from_far(0)
+            w_got(2)
+            from_end(3)
+            for j in (2, 3):
+                t_send(1, j, 0, 3, inner)
+            from_far(1)
+            w_got(3)
             w_got(4)
             w_got(5)
-            for j in (0, 1, 2):
-                t_wait(3, j)
-                t_send(4, j, 3, 3, outer)
-                go(tm[3][j])
+            from_far(2)
+            from_far(3)
+            for j in (0, 1):
+                t_send(3, j, 3, 3, outer)
+
+            def half_sums(u):
+                here = pl.ds(u * unit, unit)
+                return (ug_acc, pl.ds(u * unit, unit), units), (ug_acc, pl.ds((u + 4) * unit, unit), units), here
+
+            def products(here, o):
+                return (dot(tok[here, cols(o)], up[cols(o), units], 1, 0),
+                        dot(cot[here, cols(o)], down[units, cols(o)], 1, 1))
+
+            for u in range(3):
+                for j in Q:
+                    tm[u][j].wait_recv()
+                (ref, a, k), (_, b, _), here = half_sums(u)
+                for i, o in enumerate((fs, fx_, fy_)):
+                    pre, dh = products(here, o)
+                    if i:
+                        pre, dh = pre + ref[a, k], dh + ref[b, k]
+                    ref[a, k] = pre
+                    ref[b, k] = dh
             for q in pieces:
                 (wy if q % 2 else wx)[1][q ^ 1].wait_recv()
-            ready(0)
-            ready(1)
-            t_wait(3, 3)
-            t_send(4, 3, 3, 3, outer)
-            go(tm[3][3])
-            ready(2)
+            for u in range(3):
+                (ref, a, k), (_, b, _), here = half_sums(u)
+                pre, dh = products(here, fd_)
+                active = jnp.maximum(pre + ref[a, k], 0.0)
+                hid[here, units] = (active * active).astype(BF16)
+                dpre[here, units] = (2.0 * active * (dh + ref[b, k])).astype(BF16)
+            for j in (2, 3):
+                from_middle(j)
+                t_send(3, j, 3, 3, outer)
 
         early = pl.ds(0, 3 * unit)
         last = pl.ds(3 * unit, unit)
@@ -542,6 +586,9 @@
             for j in (1, 2, 3):
                 t_wait(3, j)
                 go(tm[3][j])
+        else:
+            ug_early(fd_, 0)
+            dg_early(fd_, 0)
         ready(3)
 
         def buf(pair, k, q):
@@ -569,14 +616,15 @@
             go(g[k][q])
 
         def terms(o, p):
-            part = last if end else slice(None)
+            split = end or o is fd_
+            part = last if split else slice(None)
             if p == 0:
                 val = dot(tok[part, cols(o)], dpre[part, units], 0, 0)
-                if end:
+                if split:
                     val = val + ug_acc[cols(o), units]
                 return val[:hd], val[hd:]
             val = dot(hid[part, units], cot[part, cols(o)], 0, 0)
-            if end:
+            if split:
                 val = val + dg_acc[units, cols(o)]
             return val[:hf], val[hf:]
 
@@ -594,7 +642,7 @@
             even, odd = terms(fy_, p)
             g_put(2, 2 * p + 1, odd)
             keep(fy_, 2 * p, even)
-        dx_block(3)
+        dx_block(3 if end else 2)
 
         def pass_on(q):
             g[0][q].wait_recv()
@@ -602,22 +650,22 @@
             ref, a, b = acc_of(o, q)
             g_put(k, q, ref[a, b] + buf(in_bufs, 0, q)[...].astype(F32))
 
-        if not end:
-            z_send(1, dx_sum(3), 3, inner)
         pass_on(0)
         pass_on(1)
         if end:
-            z_send(2, dx_sum(3), 1, across)
+            z_send(2, dx_sum(3), 4, beyond)
+        else:
+            z_send(1, dx_sum(2) + z_wait(1), 3, inner)
         for p in range(2):
             for h, v in enumerate(terms(fs, p)):
                 keep(fs, 2 * p + h, v)
         pass_on(2)
         pass_on(3)
         if not end:
-            dx_block(2)
+            dx_block(3)
             dx_block(1)
             dx_block(0)
-            z_send(0, dx_sum(2) + z_wait(1), 2, inner)
+            z_send(0, dx_sum(3), 2, inner)
             z_send(2, dx_sum(1) + z_wait(3), 0, outer)
 
         back = (remote(ug_back, ug_home, bs.at[0], br.at[0], outer),
@@ -648,11 +696,10 @@
             finish(q)
         if not end:
             go(back[1])
-            near = dx_sum(0) + z_wait(0)
-            dx_out[...] = (near + z_wait(2)).astype(BF16)
+            near = dx_sum(0) + z_wait(0) + z_wait(2)
+            dx_out[...] = (near + z_wait(4)).astype(BF16)
         else:
-            near = dx_sum(0) + z_wait(0)
-            dx_out[...] = (near + z_wait(1)).astype(BF16)
+            dx_out[...] = (dx_sum(0) + z_wait(0)).astype(BF16)
             back[0].wait_recv()
             ug_out[:, pl.ds(nown, give)] = ug_home[...].astype(F32) * factor
             back[1].wait_recv()
@@ -699,10 +746,10 @@
             V((3, 2, hf, dl), BF16), V((3, 2, hf, dl), BF16),
             V((dl, give), BF16), V((give, dl), BF16), V((dl, give), BF16), V((give, dl), BF16),
             V((4, rows, width), F32), V((4, rows, width), BF16), V((4, rows, width), BF16),
-            V((3, rows, width), BF16), V((4, rows, width), BF16),
+            V((3, rows, width), BF16), V((5, rows, width), BF16),
             dma((6,)), dma((2,)), dma((2,)), dma((2, 6)), dma((2, 6)), dma((2, 6)), dma((2, 6)),
             dma((5, 4)), dma((4, 4)), dma((4, 4)), dma((4, 4)),
-            dma((4,)), dma((4,)), dma((3,)), dma((4,)), dma((3, 4)), dma((3, 4)), dma((2,)), dma((2,)),
+            dma((4,)), dma((4,)), dma((3,)), dma((5,)), dma((3, 4)), dma((3, 4)), dma((2,)), dma((2,)),
         ],
         compiler_params=pltpu.CompilerParams(
             collective_id=0, has_side_effects=True, vmem_limit_bytes=60_000_000

time: 114 us -> 110 us (0.965)
  Pallas kernels: 113 us -> 109 us
    pallas_call x1, Pallas kernels: 111 us -> 107 us  [line_shards(): pl.pallas_call(functools.partial(line_kernel, factor, give), out_shape=(V...]
where the time goes in v3:
time: 110 us; the launch traced here: 109 us
  Pallas kernels  109 us (99%)
    pallas_call x1, Pallas kernels, line_shards(): pl.pallas_call(functools.partial(line_kernel, factor, give), out_shape=(V...  107 us

profile of v3, /device:TPU:0, one launch (start us, length us, event | category | flops | bytes accessed | tf_op | source)
XLA Modules:
  0.0 109.5 jit_solution(9869815146008137698)
XLA Ops:
  0.6 107.2 %shard_map.67 = (bf16[128,2048]{1,0:T(8,128)(2,1)S(1)}, f32[512,512]{1,0:T(8,128)S(1)}, f32[512,512]{1,0:T(8,128)S(1)}) custom-call(bf16[128,2048]{1,0:T(8,128)(2,1)} %tok_in.1, bf16[512,512]{1,0:T(8,128)(2,1)} %up_in.1, bf16[512,512]{1,0:T(8,128)(2,1)} %down_in.1, bf16[128,2048]{1,0:T(8,128)(2,1)} %cot_in.1), custom_call_target="tpu_custom_call" | custom-call | tf_op jit(solution)/shard_map/pallas_call | solution.py:734
  107.8 1.5 %shard_map.68 = (bf16[128,2048]{1,0:T(8,128)(2,1)}, f32[512,512]{1,0:T(8,128)}, f32[512,512]{1,0:T(8,128)}) custom-call(bf16[128,2048]{1,0:T(8,128)(2,1)S(1)} %get-tuple-element.6.refs_0_, f32[512,512]{1,0:T(8,128)S(1)} %get-tuple-element.7.refs_1_, f32[512,512]{1,0:T(8,128)S(1)} %get-tuple-element.8.refs_2_), custom_call_target="tpu_custom_call" | custom-call | tf_op jit(solution)/shard_map/pallas_call | solution.py:758

commit v4 on v3

--- a/solution.py
+++ b/solution.py
@@ -319,7 +319,7 @@
     dx_out, ug_out, dg_out,
     tok, cot, up, down, up_give, down_give, hid, dpre, ug_acc, dg_acc,
     ug_send, ug_recv, dg_send, dg_recv, ug_back, dg_back, ug_home, dg_home,
-    dx_own, dxm_send, dxm_recv, dxz_send, dxz_recv,
+    ue_send, ue_recv, de_send, de_recv, dx_own, dxm_send, dxm_recv, dxz_send, dxz_recv,
     local_sem, exs, exr, wxs, wxr, wys, wyr, ts, tr, tms, tmr,
     ms, mr, dzs, dzr, gs, gr, bs, br,
 ):
@@ -344,26 +344,29 @@
 
     bufs = (tok, cot)
 
+    def rows_of(j, u, shift=0):
+        return bufs[j % 2].at[pl.ds(u * unit + shift + (j // 2) * rows, hr)]
+
     def body(end):
         nf = fl - give if end else fl + give
-        hf = nf // 2
         nown = fl - give if end else fl
         units = slice(0, nf)
         locals_ = [
             pltpu.make_async_copy(up_in.at[:, pl.ds(0, nown)], up.at[cols(fs), pl.ds(0, nown)], local_sem.at[0]),
             pltpu.make_async_copy(down_in.at[pl.ds(0, nown)], down.at[pl.ds(0, nown), cols(fs)], local_sem.at[1]),
-            pltpu.make_async_copy(tok_in, tok.at[pl.ds(0, rows)], local_sem.at[2]),
-            pltpu.make_async_copy(cot_in, cot.at[pl.ds(0, rows)], local_sem.at[3]),
         ]
+        for j in Q:
+            mine = pl.ds((j // 2) * hr, hr)
+            locals_.append(pltpu.make_async_copy((tok_in, cot_in)[j % 2].at[mine], rows_of(j, 0), local_sem.at[2 + j]))
         if end:
             locals_ += [
-                pltpu.make_async_copy(up_in.at[:, pl.ds(nown, give)], up_give, local_sem.at[4]),
-                pltpu.make_async_copy(down_in.at[pl.ds(nown, give)], down_give, local_sem.at[5]),
+                pltpu.make_async_copy(up_in.at[:, pl.ds(nown, give)], up_give, local_sem.at[6]),
+                pltpu.make_async_copy(down_in.at[pl.ds(nown, give)], down_give, local_sem.at[7]),
             ]
         for cp in locals_:
             cp.start()
         barrier = pltpu.get_barrier_semaphore()
-        peers = (mate, xn, yn, inner, beyond) if end else (mate, xn, yn, inner, beyond, outer)
+        peers = (mate, xn, yn, inner) if end else (mate, xn, yn, inner, outer)
         for peer in peers:
             pl.semaphore_signal(barrier, inc=1, device_id=peer, device_id_type=MESH)
         pl.semaphore_wait(barrier, len(peers))
@@ -396,16 +399,13 @@
         wy = [[remote(piece(o, q), piece(o, q), wys.at[i, q], wyr.at[i, q], yn) for q in pieces]
               for i, o in enumerate((fs, fx_))]
 
-        def rows_of(j, u, shift=0):
-            return bufs[j % 2].at[pl.ds(u * unit + shift + (j // 2) * hr, hr)]
-
         def t_send(flow, j, u, v, peer):
             go(remote(rows_of(j, u), rows_of(j, v), ts.at[flow, j], tr.at[v, j], peer))
 
         def t_wait(u, j):
             remote(rows_of(j, u), rows_of(j, u), ts.at[0, j], tr.at[u, j], mate).wait_recv()
 
-        tm = [[remote(rows_of(j, u), rows_of(j, u, rows), tms.at[u, j], tmr.at[u, j], mate) for j in Q]
+        tm = [[remote(rows_of(j, u), rows_of(j, u, hr), tms.at[u, j], tmr.at[u, j], mate) for j in Q]
               for u in range(4)]
 
         def w_got(q):
@@ -419,8 +419,8 @@
         ex = (remote(up_give, up.at[cols(fs), pl.ds(fl, give)], exs.at[0], exr.at[0], inner),
               remote(down_give, down.at[pl.ds(fl, give), cols(fs)], exs.at[1], exr.at[1], inner))
 
-        def hidden_block(u):
-            here = pl.ds(u * unit, unit)
+        def hidden_block(u, here=None):
+            here = pl.ds(u * unit, unit) if here is None else here
             active = jnp.maximum(dot(tok[here, :], up[:, units], 1, 0), 0.0)
             hid[here, units] = (active * active).astype(BF16)
             dh = dot(cot[here, :], down[units, :], 1, 1)
@@ -434,8 +434,10 @@
             def tile(j, carry):
                 o = cols(j)
                 part = dot(dpre[here, units], up[o, units], 1, 1)
-                dx_own[u, :, o] = part[:rows]
-                dxm_send[u, :, o] = part[rows:].astype(BF16)
+                for h in range(2):
+                    half = pl.ds(h * hr, hr)
+                    dx_own[u, half, o] = part[2 * h * hr : (2 * h + 1) * hr]
+                    dxm_send[u, half, o] = part[(2 * h + 1) * hr : (2 * h + 2) * hr].astype(BF16)
                 return carry
 
             lax.fori_loop(0, 4, tile, 0)
@@ -568,8 +570,9 @@
                 from_middle(j)
                 t_send(3, j, 3, 3, outer)
 
-        early = pl.ds(0, 3 * unit)
-        last = pl.ds(3 * unit, unit)
+        cut = 3 * unit + rows if end else 3 * unit
+        early = pl.ds(0, cut)
+        last = pl.ds(cut, 4 * unit - cut)
 
         def ug_early(o, carry):
             ug_acc[cols(o), units] = dot(tok[early, cols(o)], dpre[early, units], 0, 0)
@@ -580,35 +583,52 @@
             return carry
 
         if end:
+            t_wait(3, 1)
+            go(tm[3][1])
+            dx_block(0)
+            for j in (0, 1):
+                tm[3][j].wait_recv()
+            hidden_block(3, pl.ds(3 * unit, rows))
             lax.fori_loop(0, 4, ug_early, 0)
+            t_wait(3, 2)
+            go(tm[3][2])
             lax.fori_loop(0, 4, dg_early, 0)
-            dx_block(0)
-            for j in (1, 2, 3):
-                t_wait(3, j)
-                go(tm[3][j])
+            t_wait(3, 3)
+            go(tm[3][3])
+            for j in (2, 3):
+                tm[3][j].wait_recv()
+            hidden_block(3, last)
         else:
             ug_early(fd_, 0)
             dg_early(fd_, 0)
-        ready(3)
-
-        def buf(pair, k, q):
-            up_buf, down_buf = pair
+            ready(3)
+        before = len(sends)
+
+        gh = nown // 2
+
+        def buf(bufs, k, q):
             if q < 2:
-                return up_buf.at[k, q, :, pl.ds(0, nf)]
-            return down_buf.at[k, q - 2, pl.ds(0, hf)]
-
-        out_bufs, in_bufs = (ug_send, dg_send), (ug_recv, dg_recv)
+                return bufs[0].at[k, q, :, pl.ds(0, nown)]
+            if q < 4:
+                return bufs[1].at[k, q - 2, pl.ds(0, gh)]
+            return bufs[q - 2].at[k]
+
+        out_bufs, in_bufs = (ug_send, dg_send, ue_send, de_send), (ug_recv, dg_recv, ue_recv, de_recv)
 
         def g_copy(k, q):
             over_x = k == 1 or (k == 0 and q % 2 == 0)
             return remote(buf(out_bufs, k, q), buf(in_bufs, k, q), gs.at[k, q], gr.at[k, q], xn if over_x else yn)
 
-        g = [[g_copy(k, q) for q in Q] for k in range(3)]
+        g = [[g_copy(k, q) for q in pieces] for k in range(3)]
 
         def acc_of(o, q):
             if q < 2:
-                return ug_acc, pl.ds(pl.multiple_of(o * dl + q * hd, hd), hd), units
-            return dg_acc, pl.ds((q - 2) * hf, hf), cols(o)
+                return ug_acc, pl.ds(pl.multiple_of(o * dl + q * hd, hd), hd), slice(0, nown)
+            if q < 4:
+                return dg_acc, pl.ds((q - 2) * gh, gh), cols(o)
+            if q == 4:
+                return ug_acc, cols(o), slice(nown, nf)
+            return dg_acc, slice(nown, nf), cols(o)
 
         def g_put(k, q, value):
             dst = buf(out_bufs, k, q)
@@ -618,31 +638,43 @@
         def terms(o, p):
             split = end or o is fd_
             part = last if split else slice(None)
-            if p == 0:
-                val = dot(tok[part, cols(o)], dpre[part, units], 0, 0)
+            few = slice(nown, nf) if p > 1 else slice(0, nown)
+            if p % 2 == 0:
+                val = dot(tok[part, cols(o)], dpre[part, few], 0, 0)
                 if split:
-                    val = val + ug_acc[cols(o), units]
-                return val[:hd], val[hd:]
-            val = dot(hid[part, units], cot[part, cols(o)], 0, 0)
+                    val = val + ug_acc[cols(o), few]
+                return (val,) if p > 1 else (val[:hd], val[hd:])
+            val = dot(hid[part, few], cot[part, cols(o)], 0, 0)
             if split:
-                val = val + dg_acc[units, cols(o)]
-            return val[:hf], val[hf:]
+                val = val + dg_acc[few, cols(o)]
+            return (val,) if p > 1 else (val[:gh], val[gh:])
 
         def keep(o, q, value):
             ref, a, b = acc_of(o, q)
             ref[a, b] = value
 
-        for p in range(2):
+        def begin(p):
+            q = 2 * p if p < 2 else p + 2
             for h, v in enumerate(terms(fd_, p)):
-                g_put(0, 2 * p + h, v)
-        for p in range(2):
-            even, odd = terms(fx_, p)
-            g_put(1, 2 * p, even)
-            keep(fx_, 2 * p + 1, odd)
-            even, odd = terms(fy_, p)
-            g_put(2, 2 * p + 1, odd)
-            keep(fy_, 2 * p, even)
-        dx_block(3 if end else 2)
+                g_put(0, q + h, v)
+
+        def follow(p):
+            q = 2 * p if p < 2 else p + 2
+            for h, v in enumerate(terms(fx_, p)):
+                if (q + h) % 2 == 0:
+                    g_put(1, q + h, v)
+                else:
+                    keep(fx_, q + h, v)
+            for h, v in enumerate(terms(fy_, p)):
+                if (q + h) % 2:
+                    g_put(2, q + h, v)
+                else:
+                    keep(fy_, q + h, v)
+
+        def own_terms(p):
+            q = 2 * p if p < 2 else p + 2
+            for h, v in enumerate(terms(fs, p)):
+                keep(fs, q + h, v)
 
         def pass_on(q):
             g[0][q].wait_recv()
@@ -650,60 +682,81 @@
             ref, a, b = acc_of(o, q)
             g_put(k, q, ref[a, b] + buf(in_bufs, 0, q)[...].astype(F32))
 
-        pass_on(0)
-        pass_on(1)
-        if end:
-            z_send(2, dx_sum(3), 4, beyond)
-        else:
-            z_send(1, dx_sum(2) + z_wait(1), 3, inner)
-        for p in range(2):
-            for h, v in enumerate(terms(fs, p)):
-                keep(fs, 2 * p + h, v)
-        pass_on(2)
-        pass_on(3)
-        if not end:
-            dx_block(3)
-            dx_block(1)
-            dx_block(0)
-            z_send(0, dx_sum(3), 2, inner)
-            z_send(2, dx_sum(1) + z_wait(3), 0, outer)
-
         back = (remote(ug_back, ug_home, bs.at[0], br.at[0], outer),
                 remote(dg_back, dg_home, bs.at[1], br.at[1], outer))
 
-        def finish(q):
+        def summed(q):
             ref, a, b = acc_of(fs, q)
             total = ref[a, b]
             for k in (1, 2):
                 g[k][q].wait_recv()
                 total = total + buf(in_bufs, k, q)[...].astype(F32)
+            return total
+
+        def finish(q):
             if q < 2:
-                r = pl.ds(q * hd, hd)
-                ug_out[r, pl.ds(0, nown)] = total[:, :nown] * factor
-                if not end:
-                    ug_back[r, :] = total[:, nown:].astype(BF16)
+                ug_out[pl.ds(q * hd, hd), pl.ds(0, nown)] = summed(q) * factor
             else:
-                n = min(nown - (q - 2) * hf, hf)
-                dg_out[pl.ds((q - 2) * hf, n), :] = total[:n] * factor
-                if n < hf:
-                    dg_back[...] = total[n:].astype(BF16)
-
-        for q in (0, 1):
-            finish(q)
-        if not end:
-            go(back[0])
-        for q in (2, 3):
-            finish(q)
-        if not end:
-            go(back[1])
-            near = dx_sum(0) + z_wait(0) + z_wait(2)
-            dx_out[...] = (near + z_wait(4)).astype(BF16)
-        else:
+                dg_out[pl.ds((q - 2) * gh, gh), :] = summed(q) * factor
+
+        if end:
+            begin(0)
+            begin(1)
+            follow(0)
+            follow(1)
+            dx_block(3)
+            pass_on(0)
+            pass_on(1)
+            own_terms(0)
+            own_terms(1)
+            pass_on(2)
+            pass_on(3)
+            z_send(2, dx_sum(3), 4, beyond)
+            for cp in sends[:before]:
+                cp.wait_send()
             dx_out[...] = (dx_sum(0) + z_wait(0)).astype(BF16)
             back[0].wait_recv()
             ug_out[:, pl.ds(nown, give)] = ug_home[...].astype(F32) * factor
             back[1].wait_recv()
             dg_out[pl.ds(nown, give), :] = dg_home[...].astype(F32) * factor
+        else:
+            begin(2)
+            begin(3)
+            follow(2)
+            follow(3)
+            dx_block(3)
+            begin(0)
+            begin(1)
+            z_send(0, dx_sum(3), 2, inner)
+            pass_on(4)
+            pass_on(5)
+            follow(0)
+            follow(1)
+            dx_block(2)
+            own_terms(2)
+            own_terms(3)
+            pass_on(0)
+            pass_on(1)
+            z_send(1, dx_sum(2) + z_wait(1), 3, inner)
+            own_terms(0)
+            own_terms(1)
+            pass_on(2)
+            pass_on(3)
+            dx_block(1)
+            dx_block(0)
+            ug_back[...] = summed(4).astype(BF16)
+            dg_back[...] = summed(5).astype(BF16)
+            for cp in sends[:before]:
+                cp.wait_send()
+            go(back[0])
+            go(back[1])
+            z_send(2, dx_sum(1) + z_wait(3), 0, outer)
+        for q in Q:
+            finish(q)
+        if not end:
+            near = dx_sum(0) + z_wait(0) + z_wait(2)
+            dx_out[...] = (near + z_wait(4)).astype(BF16)
+        del sends[:before]
         for cp in sends:
             cp.wait_send()
 
@@ -726,7 +779,7 @@
     mine = ntp * rows
     give = fl // 4
     most = fl + give
-    hd, hf = dl // 2, most // 2
+    hd = dl // 2
     dma = pltpu.SemaphoreType.DMA
     any_space = pl.BlockSpec(memory_space=pl.ANY)
     vmem = pl.BlockSpec(memory_space=pltpu.VMEM)
@@ -742,14 +795,15 @@
             V((dl, give), BF16), V((give, dl), BF16),
             V((mine, most), BF16), V((mine, most), BF16),
             V((width, most), F32), V((most, width), F32),
-            V((3, 2, hd, most), BF16), V((3, 2, hd, most), BF16),
-            V((3, 2, hf, dl), BF16), V((3, 2, hf, dl), BF16),
+            V((3, 2, hd, fl), BF16), V((3, 2, hd, fl), BF16),
+            V((3, 2, fl // 2, dl), BF16), V((3, 2, fl // 2, dl), BF16),
             V((dl, give), BF16), V((give, dl), BF16), V((dl, give), BF16), V((give, dl), BF16),
+            V((3, dl, give), BF16), V((3, dl, give), BF16), V((3, give, dl), BF16), V((3, give, dl), BF16),
             V((4, rows, width), F32), V((4, rows, width), BF16), V((4, rows, width), BF16),
             V((3, rows, width), BF16), V((5, rows, width), BF16),
-            dma((6,)), dma((2,)), dma((2,)), dma((2, 6)), dma((2, 6)), dma((2, 6)), dma((2, 6)),
+            dma((8,)), dma((2,)), dma((2,)), dma((2, 6)), dma((2, 6)), dma((2, 6)), dma((2, 6)),
             dma((5, 4)), dma((4, 4)), dma((4, 4)), dma((4, 4)),
-            dma((4,)), dma((4,)), dma((3,)), dma((5,)), dma((3, 4)), dma((3, 4)), dma((2,)), dma((2,)),
+            dma((4,)), dma((4,)), dma((3,)), dma((5,)), dma((3, 6)), dma((3, 6)), dma((2,)), dma((2,)),
         ],
         compiler_params=pltpu.CompilerParams(
             collective_id=0, has_side_effects=True, vmem_limit_bytes=60_000_000

time: 110 us -> 107 us (0.973)
  Pallas kernels: 109 us -> 105 us
    pallas_call x1, Pallas kernels: 107 us -> 104 us  [line_shards(): pl.pallas_call(functools.partial(line_kernel, factor, give), out_shape=(V...]
where the time goes in v4:
time: 107 us; the launch traced here: 106 us
  Pallas kernels  105 us (98%)
    pallas_call x1, Pallas kernels, line_shards(): pl.pallas_call(functools.partial(line_kernel, factor, give), out_shape=(V...  104 us

profile of v4, /device:TPU:0, one launch (start us, length us, event | category | flops | bytes accessed | tf_op | source)
XLA Modules:
  0.0 106.2 jit_solution(11277792345632659351)
XLA Ops:
  0.6 103.9 %shard_map.67 = (bf16[128,2048]{1,0:T(8,128)(2,1)S(1)}, f32[512,512]{1,0:T(8,128)S(1)}, f32[512,512]{1,0:T(8,128)S(1)}) custom-call(bf16[128,2048]{1,0:T(8,128)(2,1)} %tok_in.1, bf16[512,512]{1,0:T(8,128)(2,1)} %up_in.1, bf16[512,512]{1,0:T(8,128)(2,1)} %down_in.1, bf16[128,2048]{1,0:T(8,128)(2,1)} %cot_in.1), custom_call_target="tpu_custom_call" | custom-call | tf_op jit(solution)/shard_map/pallas_call | solution.py:787
  104.5 1.5 %shard_map.68 = (bf16[128,2048]{1,0:T(8,128)(2,1)}, f32[512,512]{1,0:T(8,128)}, f32[512,512]{1,0:T(8,128)}) custom-call(bf16[128,2048]{1,0:T(8,128)(2,1)S(1)} %get-tuple-element.6.refs_0_, f32[512,512]{1,0:T(8,128)S(1)} %get-tuple-element.7.refs_1_, f32[512,512]{1,0:T(8,128)S(1)} %get-tuple-element.8.refs_2_), custom_call_target="tpu_custom_call" | custom-call | tf_op jit(solution)/shard_map/pallas_call | solution.py:812

commit v5 on v4

--- a/solution.py
+++ b/solution.py
@@ -373,8 +373,6 @@
         for cp in locals_:
             cp.wait()
 
-        sends = []
-
         def remote(src, dst, s, r, peer):
             return pltpu.make_async_remote_copy(
                 src_ref=src, dst_ref=dst, send_sem=s, recv_sem=r, device_id=peer, device_id_type=MESH
@@ -382,7 +380,12 @@
 
         def go(cp):
             cp.start()
-            sends.append(cp)
+
+        def sent(ref, sem):
+            remote(ref, ref, sem, sem, mate).wait_send()
+
+        def size(elements):
+            return tok.at[pl.ds(0, elements // width)]
 
         def piece(o, q):
             if q < 2:
@@ -394,19 +397,26 @@
             return down.at[pl.ds(fl, give), cols(o)]
 
         pieces = Q if end else range(6)
-        wx = [[remote(piece(o, q), piece(o, q), wxs.at[i, q], wxr.at[i, q], xn) for q in pieces]
+        wx = [[remote(piece(o, q), piece(o, q), wxs.at[0], wxr.at[i, q], xn) for q in pieces]
               for i, o in enumerate((fs, fy_))]
-        wy = [[remote(piece(o, q), piece(o, q), wys.at[i, q], wyr.at[i, q], yn) for q in pieces]
+        wy = [[remote(piece(o, q), piece(o, q), wys.at[0], wyr.at[i, q], yn) for q in pieces]
               for i, o in enumerate((fs, fx_))]
 
         def t_send(flow, j, u, v, peer):
-            go(remote(rows_of(j, u), rows_of(j, v), ts.at[flow, j], tr.at[v, j], peer))
+            go(remote(rows_of(j, u), rows_of(j, v), ts.at[flow], tr.at[v, j], peer))
 
         def t_wait(u, j):
-            remote(rows_of(j, u), rows_of(j, u), ts.at[0, j], tr.at[u, j], mate).wait_recv()
-
-        tm = [[remote(rows_of(j, u), rows_of(j, u, hr), tms.at[u, j], tmr.at[u, j], mate) for j in Q]
+            remote(rows_of(j, u), rows_of(j, u), ts.at[0], tr.at[u, j], mate).wait_recv()
+
+        def mate_slot(u, j):
+            return 2 * u + j // 2 + (end and u == 3 and j == 3)
+
+        tm = [[remote(rows_of(j, u), rows_of(j, u, hr), tms.at[0], tmr.at[mate_slot(u, j)], mate) for j in Q]
               for u in range(4)]
+
+        def from_mate(u, h):
+            got = pl.ds(u * unit, hr if end and u == 3 and h else rows)
+            remote(tok.at[got], tok.at[got], tms.at[0], tmr.at[2 * u + h], mate).wait_recv()
 
         def w_got(q):
             wx[0][q].wait_recv()
@@ -426,7 +436,7 @@
             dh = dot(cot[here, :], down[units, :], 1, 1)
             dpre[here, units] = (2.0 * active * dh).astype(BF16)
 
-        dxm = [remote(dxm_send.at[u], dxm_recv.at[u], ms.at[u], mr.at[u], mate) for u in range(4)]
+        dxm = [remote(dxm_send.at[u], dxm_recv.at[u], ms.at[0], mr.at[u], mate) for u in range(4)]
 
         def dx_block(u):
             here = pl.ds(u * unit, unit)
@@ -453,11 +463,11 @@
 
         def z_send(i, value, slot, peer):
             dxz_send[i] = value.astype(BF16)
-            go(remote(dxz_send.at[i], dxz_recv.at[slot], dzs.at[i], dzr.at[slot], peer))
+            go(remote(dxz_send.at[i], dxz_recv.at[slot], dzs.at[0], dzr.at[slot], peer))
 
         def ready(u):
-            for j in Q:
-                tm[u][j].wait_recv()
+            from_mate(u, 0)
+            from_mate(u, 1)
             hidden_block(u)
 
         if end:
@@ -540,37 +550,35 @@
             for j in (0, 1):
                 t_send(3, j, 3, 3, outer)
 
-            def half_sums(u):
-                here = pl.ds(u * unit, unit)
-                return (ug_acc, pl.ds(u * unit, unit), units), (ug_acc, pl.ds((u + 4) * unit, unit), units), here
-
             def products(here, o):
                 return (dot(tok[here, cols(o)], up[cols(o), units], 1, 0),
                         dot(cot[here, cols(o)], down[units, cols(o)], 1, 1))
 
-            for u in range(3):
-                for j in Q:
-                    tm[u][j].wait_recv()
-                (ref, a, k), (_, b, _), here = half_sums(u)
+            spans = [(u * unit, unit) for u in range(3)] + [(3 * unit, rows)]
+            for u, (at, n) in enumerate(spans):
+                here, there = pl.ds(at, n), pl.ds(4 * unit + at, n)
+                from_mate(u, 0)
+                if u < 3:
+                    from_mate(u, 1)
                 for i, o in enumerate((fs, fx_, fy_)):
                     pre, dh = products(here, o)
                     if i:
-                        pre, dh = pre + ref[a, k], dh + ref[b, k]
-                    ref[a, k] = pre
-                    ref[b, k] = dh
+                        pre, dh = pre + ug_acc[here, units], dh + ug_acc[there, units]
+                    ug_acc[here, units] = pre
+                    ug_acc[there, units] = dh
             for q in pieces:
                 (wy if q % 2 else wx)[1][q ^ 1].wait_recv()
-            for u in range(3):
-                (ref, a, k), (_, b, _), here = half_sums(u)
+            for at, n in spans:
+                here, there = pl.ds(at, n), pl.ds(4 * unit + at, n)
                 pre, dh = products(here, fd_)
-                active = jnp.maximum(pre + ref[a, k], 0.0)
+                active = jnp.maximum(pre + ug_acc[here, units], 0.0)
                 hid[here, units] = (active * active).astype(BF16)
-                dpre[here, units] = (2.0 * active * (dh + ref[b, k])).astype(BF16)
+                dpre[here, units] = (2.0 * active * (dh + ug_acc[there, units])).astype(BF16)
             for j in (2, 3):
                 from_middle(j)
                 t_send(3, j, 3, 3, outer)
 
-        cut = 3 * unit + rows if end else 3 * unit
+        cut = 3 * unit + rows
         early = pl.ds(0, cut)
         last = pl.ds(cut, 4 * unit - cut)
 
@@ -586,23 +594,38 @@
             t_wait(3, 1)
             go(tm[3][1])
             dx_block(0)
-            for j in (0, 1):
-                tm[3][j].wait_recv()
+            from_mate(3, 0)
             hidden_block(3, pl.ds(3 * unit, rows))
             lax.fori_loop(0, 4, ug_early, 0)
             t_wait(3, 2)
             go(tm[3][2])
             lax.fori_loop(0, 4, dg_early, 0)
+            from_mate(3, 1)
+            spare = pl.ds(fl, rows)
+            active = jnp.maximum(dot(tok[last, :], up[:, units], 1, 0), 0.0)
+            hid[last, units] = (active * active).astype(BF16)
+            dg_acc[spare, units] = active
             t_wait(3, 3)
             go(tm[3][3])
-            for j in (2, 3):
-                tm[3][j].wait_recv()
-            hidden_block(3, last)
+            from_mate(3, 2)
+            dh = dot(cot[last, :], down[units, :], 1, 1)
+            dpre[last, units] = (2.0 * dg_acc[spare, units] * dh).astype(BF16)
         else:
             ug_early(fd_, 0)
             dg_early(fd_, 0)
-            ready(3)
-        before = len(sends)
+            from_mate(3, 1)
+            hidden_block(3, last)
+
+        def drain():
+            w_bytes = (dl * nown * 2) * 3 // 2 + (0 if end else dl * give * 3)
+            sent(size(w_bytes), wxs.at[0])
+            sent(size(w_bytes), wys.at[0])
+            for flow in range(1 if end else 5):
+                sent(tok.at[pl.ds(0, unit)], ts.at[flow])
+            sent(tok, tms.at[0])
+            if end:
+                for cp in ex:
+                    cp.wait_send()
 
         gh = nown // 2
 
@@ -617,7 +640,7 @@
 
         def g_copy(k, q):
             over_x = k == 1 or (k == 0 and q % 2 == 0)
-            return remote(buf(out_bufs, k, q), buf(in_bufs, k, q), gs.at[k, q], gr.at[k, q], xn if over_x else yn)
+            return remote(buf(out_bufs, k, q), buf(in_bufs, k, q), gs.at[0], gr.at[k, q], xn if over_x else yn)
 
         g = [[g_copy(k, q) for q in pieces] for k in range(3)]
 
@@ -712,8 +735,7 @@
             pass_on(2)
             pass_on(3)
             z_send(2, dx_sum(3), 4, beyond)
-            for cp in sends[:before]:
-                cp.wait_send()
+            drain()
             dx_out[...] = (dx_sum(0) + z_wait(0)).astype(BF16)
             back[0].wait_recv()
             ug_out[:, pl.ds(nown, give)] = ug_home[...].astype(F32) * factor
@@ -746,8 +768,7 @@
             dx_block(0)
             ug_back[...] = summed(4).astype(BF16)
             dg_back[...] = summed(5).astype(BF16)
-            for cp in sends[:before]:
-                cp.wait_send()
+            drain()
             go(back[0])
             go(back[1])
             z_send(2, dx_sum(1) + z_wait(3), 0, outer)
@@ -756,9 +777,13 @@
         if not end:
             near = dx_sum(0) + z_wait(0) + z_wait(2)
             dx_out[...] = (near + z_wait(4)).astype(BF16)
-        del sends[:before]
-        for cp in sends:
-            cp.wait_send()
+        g_bytes = 12 * hd * nown + (0 if end else 6 * dl * give)
+        sent(size(g_bytes), gs.at[0])
+        sent(dxm_send, ms.at[0])
+        sent(dxz_send, dzs.at[0])
+        if not end:
+            for cp in back:
+                cp.wait_send()
 
     pl.when(at_end)(lambda: body(True))
     pl.when(jnp.logical_not(at_end))(lambda: body(False))
@@ -801,9 +826,9 @@
             V((3, dl, give), BF16), V((3, dl, give), BF16), V((3, give, dl), BF16), V((3, give, dl), BF16),
             V((4, rows, width), F32), V((4, rows, width), BF16), V((4, rows, width), BF16),
             V((3, rows, width), BF16), V((5, rows, width), BF16),
-            dma((8,)), dma((2,)), dma((2,)), dma((2, 6)), dma((2, 6)), dma((2, 6)), dma((2, 6)),
-            dma((5, 4)), dma((4, 4)), dma((4, 4)), dma((4, 4)),
-            dma((4,)), dma((4,)), dma((3,)), dma((5,)), dma((3, 6)), dma((3, 6)), dma((2,)), dma((2,)),
+            dma((8,)), dma((2,)), dma((2,)), dma((1,)), dma((2, 6)), dma((1,)), dma((2, 6)),
+            dma((5,)), dma((4, 4)), dma((1,)), dma((9,)),
+            dma((1,)), dma((4,)), dma((1,)), dma((5,)), dma((1,)), dma((3, 6)), dma((2,)), dma((2,)),
         ],
         compiler_params=pltpu.CompilerParams(
             collective_id=0, has_side_effects=True, vmem_limit_bytes=60_000_000

time: 107 us -> 106 us (level)
  no operation moved by 1% of the time
where the time goes in v5:
time: 106 us; the launch traced here: 105 us
  Pallas kernels  104 us (98%)
    pallas_call x1, Pallas kernels, line_shards(): pl.pallas_call(functools.partial(line_kernel, factor, give), out_shape=(V...  103 us

profile of v5, /device:TPU:0, one launch (start us, length us, event | category | flops | bytes accessed | tf_op | source)
XLA Modules:
  0.0 105.2 jit_solution(16590792523884577259)
XLA Ops:
  0.6 102.9 %shard_map.67 = (bf16[128,2048]{1,0:T(8,128)(2,1)S(1)}, f32[512,512]{1,0:T(8,128)S(1)}, f32[512,512]{1,0:T(8,128)S(1)}) custom-call(bf16[128,2048]{1,0:T(8,128)(2,1)} %tok_in.1, bf16[512,512]{1,0:T(8,128)(2,1)} %up_in.1, bf16[512,512]{1,0:T(8,128)(2,1)} %down_in.1, bf16[128,2048]{1,0:T(8,128)(2,1)} %cot_in.1), custom_call_target="tpu_custom_call" | custom-call | tf_op jit(solution)/shard_map/pallas_call | solution.py:812
  103.5 1.5 %shard_map.68 = (bf16[128,2048]{1,0:T(8,128)(2,1)}, f32[512,512]{1,0:T(8,128)}, f32[512,512]{1,0:T(8,128)}) custom-call(bf16[128,2048]{1,0:T(8,128)(2,1)S(1)} %get-tuple-element.6.refs_0_, f32[512,512]{1,0:T(8,128)S(1)} %get-tuple-element.7.refs_1_, f32[512,512]{1,0:T(8,128)S(1)} %get-tuple-element.8.refs_2_), custom_call_target="tpu_custom_call" | custom-call | tf_op jit(solution)/shard_map/pallas_call | solution.py:837

commit v6 on v5

--- a/solution.py
+++ b/solution.py
@@ -321,7 +321,7 @@
     ug_send, ug_recv, dg_send, dg_recv, ug_back, dg_back, ug_home, dg_home,
     ue_send, ue_recv, de_send, de_recv, dx_own, dxm_send, dxm_recv, dxz_send, dxz_recv,
     local_sem, exs, exr, wxs, wxr, wys, wyr, ts, tr, tms, tmr,
-    ms, mr, dzs, dzr, gs, gr, bs, br,
+    ms, mr, dzs, dzr, gs, gr, bs, br, held, hs, hr_, vs, vr,
 ):
     fs, tp = lax.axis_index("fs"), lax.axis_index("tp")
     rows, width = tok_in.shape
@@ -638,9 +638,25 @@
 
         out_bufs, in_bufs = (ug_send, dg_send, ue_send, de_send), (ug_recv, dg_recv, ue_recv, de_recv)
 
+        detours = ((1, 2), (2, 3))
+        few_rows = give // 2
+
         def g_copy(k, q):
             over_x = k == 1 or (k == 0 and q % 2 == 0)
-            return remote(buf(out_bufs, k, q), buf(in_bufs, k, q), gs.at[0], gr.at[k, q], xn if over_x else yn)
+            src, dst = buf(out_bufs, k, q), buf(in_bufs, k, q)
+            if end and (k, q) in detours:
+                most = pl.ds(0, gh - few_rows)
+                src, dst = src.at[most], dst.at[most]
+            return remote(src, dst, gs.at[0], gr.at[k, q], xn if over_x else yn)
+
+        def rest_of(bufs, i):
+            k, q = detours[i]
+            return bufs[1].at[k, q - 2, pl.ds((fl - give) // 2 - few_rows, few_rows)]
+
+        there = 2 * (z + toward) + c
+        leave = [remote(rest_of(out_bufs, i), held.at[i], hs.at[i], hr_.at[i], ((fx_, fy_)[i], there))
+                 for i in range(2)]
+        arrive = [remote(held.at[i], rest_of(in_bufs, i), vs.at[i], vr.at[i], outer) for i in range(2)]
 
         g = [[g_copy(k, q) for q in pieces] for k in range(3)]
 
@@ -657,6 +673,8 @@
             dst = buf(out_bufs, k, q)
             dst[...] = value.astype(BF16)
             go(g[k][q])
+            if end and (k, q) in detours:
+                go(leave[detours.index((k, q))])
 
         def terms(o, p):
             split = end or o is fd_
@@ -713,6 +731,8 @@
             total = ref[a, b]
             for k in (1, 2):
                 g[k][q].wait_recv()
+                if end and (k, q) in detours:
+                    arrive[detours.index((k, q))].wait_recv()
                 total = total + buf(in_bufs, k, q)[...].astype(F32)
             return total
 
@@ -772,18 +792,20 @@
             go(back[0])
             go(back[1])
             z_send(2, dx_sum(1) + z_wait(3), 0, outer)
+            for i in range(2):
+                leave[i].wait_recv()
+                go(arrive[i])
         for q in Q:
             finish(q)
         if not end:
             near = dx_sum(0) + z_wait(0) + z_wait(2)
             dx_out[...] = (near + z_wait(4)).astype(BF16)
-        g_bytes = 12 * hd * nown + (0 if end else 6 * dl * give)
+        g_bytes = 12 * hd * nown + (-2 * few_rows * dl if end else 6 * dl * give)
         sent(size(g_bytes), gs.at[0])
         sent(dxm_send, ms.at[0])
         sent(dxz_send, dzs.at[0])
-        if not end:
-            for cp in back:
-                cp.wait_send()
+        for cp in leave if end else (*back, *arrive):
+            cp.wait_send()
 
     pl.when(at_end)(lambda: body(True))
     pl.when(jnp.logical_not(at_end))(lambda: body(False))
@@ -829,6 +851,7 @@
             dma((8,)), dma((2,)), dma((2,)), dma((1,)), dma((2, 6)), dma((1,)), dma((2, 6)),
             dma((5,)), dma((4, 4)), dma((1,)), dma((9,)),
             dma((1,)), dma((4,)), dma((1,)), dma((5,)), dma((1,)), dma((3, 6)), dma((2,)), dma((2,)),
+            V((2, give // 2, dl), BF16), dma((2,)), dma((2,)), dma((2,)), dma((2,)),
         ],
         compiler_params=pltpu.CompilerParams(
             collective_id=0, has_side_effects=True, vmem_limit_bytes=60_000_000

time: 106 us -> 104 us (0.981)
    pallas_call x1, Pallas kernels: 103 us -> 102 us  [line_shards(): pl.pallas_call(functools.partial(line_kernel, factor, give), out_shape=(V...]
where the time goes in v6:
time: 104 us
  Pallas kernels  103 us (99%)
    pallas_call x1, Pallas kernels, line_shards(): pl.pallas_call(functools.partial(line_kernel, factor, give), out_shape=(V...  102 us

profile of v6, /device:TPU:0, one launch (start us, length us, event | category | flops | bytes accessed | tf_op | source)
XLA Modules:
  0.0 103.9 jit_solution(15938718115653796397)
XLA Ops:
  0.6 101.6 %shard_map.67 = (bf16[128,2048]{1,0:T(8,128)(2,1)S(1)}, f32[512,512]{1,0:T(8,128)S(1)}, f32[512,512]{1,0:T(8,128)S(1)}) custom-call(bf16[128,2048]{1,0:T(8,128)(2,1)} %tok_in.1, bf16[512,512]{1,0:T(8,128)(2,1)} %up_in.1, bf16[512,512]{1,0:T(8,128)(2,1)} %down_in.1, bf16[128,2048]{1,0:T(8,128)(2,1)} %cot_in.1), custom_call_target="tpu_custom_call" | custom-call | tf_op jit(solution)/shard_map/pallas_call | solution.py:834
  102.2 1.5 %shard_map.68 = (bf16[128,2048]{1,0:T(8,128)(2,1)}, f32[512,512]{1,0:T(8,128)}, f32[512,512]{1,0:T(8,128)}) custom-call(bf16[128,2048]{1,0:T(8,128)(2,1)S(1)} %get-tuple-element.6.refs_0_, f32[512,512]{1,0:T(8,128)S(1)} %get-tuple-element.7.refs_1_, f32[512,512]{1,0:T(8,128)S(1)} %get-tuple-element.8.refs_2_), custom_call_target="tpu_custom_call" | custom-call | tf_op jit(solution)/shard_map/pallas_call | solution.py:860

commit v7 on v6

--- a/solution.py
+++ b/solution.py
@@ -353,15 +353,15 @@
         units = slice(0, nf)
         locals_ = [
             pltpu.make_async_copy(up_in.at[:, pl.ds(0, nown)], up.at[cols(fs), pl.ds(0, nown)], local_sem.at[0]),
-            pltpu.make_async_copy(down_in.at[pl.ds(0, nown)], down.at[pl.ds(0, nown), cols(fs)], local_sem.at[1]),
+            pltpu.make_async_copy(down_in.at[pl.ds(0, nown)], down.at[pl.ds(0, nown), cols(fs)], local_sem.at[0]),
         ]
         for j in Q:
             mine = pl.ds((j // 2) * hr, hr)
-            locals_.append(pltpu.make_async_copy((tok_in, cot_in)[j % 2].at[mine], rows_of(j, 0), local_sem.at[2 + j]))
+            locals_.append(pltpu.make_async_copy((tok_in, cot_in)[j % 2].at[mine], rows_of(j, 0), local_sem.at[0]))
         if end:
             locals_ += [
-                pltpu.make_async_copy(up_in.at[:, pl.ds(nown, give)], up_give, local_sem.at[6]),
-                pltpu.make_async_copy(down_in.at[pl.ds(nown, give)], down_give, local_sem.at[7]),
+                pltpu.make_async_copy(up_in.at[:, pl.ds(nown, give)], up_give, local_sem.at[0]),
+                pltpu.make_async_copy(down_in.at[pl.ds(nown, give)], down_give, local_sem.at[0]),
             ]
         for cp in locals_:
             cp.start()
@@ -370,8 +370,8 @@
         for peer in peers:
             pl.semaphore_signal(barrier, inc=1, device_id=peer, device_id_type=MESH)
         pl.semaphore_wait(barrier, len(peers))
-        for cp in locals_:
-            cp.wait()
+        taken = tok.at[pl.ds(0, 2 * (dl * fl + rows * width) // width)]
+        pltpu.make_async_copy(taken, taken, local_sem.at[0]).wait()
 
         def remote(src, dst, s, r, peer):
             return pltpu.make_async_remote_copy(
@@ -397,9 +397,9 @@
             return down.at[pl.ds(fl, give), cols(o)]
 
         pieces = Q if end else range(6)
-        wx = [[remote(piece(o, q), piece(o, q), wxs.at[0], wxr.at[i, q], xn) for q in pieces]
+        wx = [[remote(piece(o, q), piece(o, q), wxs.at[0], wxr.at[6 if i else q], xn) for q in pieces]
               for i, o in enumerate((fs, fy_))]
-        wy = [[remote(piece(o, q), piece(o, q), wys.at[0], wyr.at[i, q], yn) for q in pieces]
+        wy = [[remote(piece(o, q), piece(o, q), wys.at[0], wyr.at[6 if i else q], yn) for q in pieces]
               for i, o in enumerate((fs, fx_))]
 
         def t_send(flow, j, u, v, peer):
@@ -417,6 +417,11 @@
         def from_mate(u, h):
             got = pl.ds(u * unit, hr if end and u == 3 and h else rows)
             remote(tok.at[got], tok.at[got], tms.at[0], tmr.at[2 * u + h], mate).wait_recv()
+
+        def passed_on():
+            ref = size(hd * nown + (nown // 2) * dl + (0 if end else give * dl))
+            for sem in (wxr.at[6], wyr.at[6]):
+                remote(ref, ref, sem, sem, mate).wait_recv()
 
         def w_got(q):
             wx[0][q].wait_recv()
@@ -484,8 +489,7 @@
                 w_got(j)
                 t_wait(1, j)
                 go(tm[1][j])
-            for q in Q:
-                (wy if q % 2 else wx)[1][q ^ 1].wait_recv()
+            passed_on()
             ready(0)
             ready(1)
             dx_block(1)
@@ -566,8 +570,7 @@
                         pre, dh = pre + ug_acc[here, units], dh + ug_acc[there, units]
                     ug_acc[here, units] = pre
                     ug_acc[there, units] = dh
-            for q in pieces:
-                (wy if q % 2 else wx)[1][q ^ 1].wait_recv()
+            passed_on()
             for at, n in spans:
                 here, there = pl.ds(at, n), pl.ds(4 * unit + at, n)
                 pre, dh = products(here, fd_)
@@ -848,7 +851,7 @@
             V((3, dl, give), BF16), V((3, dl, give), BF16), V((3, give, dl), BF16), V((3, give, dl), BF16),
             V((4, rows, width), F32), V((4, rows, width), BF16), V((4, rows, width), BF16),
             V((3, rows, width), BF16), V((5, rows, width), BF16),
-            dma((8,)), dma((2,)), dma((2,)), dma((1,)), dma((2, 6)), dma((1,)), dma((2, 6)),
+            dma((1,)), dma((2,)), dma((2,)), dma((1,)), dma((7,)), dma((1,)), dma((7,)),
             dma((5,)), dma((4, 4)), dma((1,)), dma((9,)),
             dma((1,)), dma((4,)), dma((1,)), dma((5,)), dma((1,)), dma((3, 6)), dma((2,)), dma((2,)),
             V((2, give // 2, dl), BF16), dma((2,)), dma((2,)), dma((2,)), dma((2,)),

time: 104 us -> 104 us (level)
  no operation moved by 1% of the time
where the time goes in v7:
time: 104 us
  Pallas kernels  103 us (99%)
    pallas_call x1, Pallas kernels, line_shards(): pl.pallas_call(functools.partial(line_kernel, factor, give), out_shape=(V...  101 us

profile of v7, /device:TPU:0, one launch (start us, length us, event | category | flops | bytes accessed | tf_op | source)
XLA Modules:
  0.0 103.7 jit_solution(15215610871608166339)
XLA Ops:
  0.6 101.4 %shard_map.67 = (bf16[128,2048]{1,0:T(8,128)(2,1)S(1)}, f32[512,512]{1,0:T(8,128)S(1)}, f32[512,512]{1,0:T(8,128)S(1)}) custom-call(bf16[128,2048]{1,0:T(8,128)(2,1)} %tok_in.1, bf16[512,512]{1,0:T(8,128)(2,1)} %up_in.1, bf16[512,512]{1,0:T(8,128)(2,1)} %down_in.1, bf16[128,2048]{1,0:T(8,128)(2,1)} %cot_in.1), custom_call_target="tpu_custom_call" | custom-call | tf_op jit(solution)/shard_map/pallas_call | solution.py:837
  102.1 1.5 %shard_map.68 = (bf16[128,2048]{1,0:T(8,128)(2,1)}, f32[512,512]{1,0:T(8,128)}, f32[512,512]{1,0:T(8,128)}) custom-call(bf16[128,2048]{1,0:T(8,128)(2,1)S(1)} %get-tuple-element.6.refs_0_, f32[512,512]{1,0:T(8,128)S(1)} %get-tuple-element.7.refs_1_, f32[512,512]{1,0:T(8,128)S(1)} %get-tuple-element.8.refs_2_), custom_call_target="tpu_custom_call" | custom-call | tf_op jit(solution)/shard_map/pallas_call | solution.py:863
